TPU v7x, 128 devices: a whole 4x4x4 slice. The times are simulated.
128 devices in a mesh: rep: 4 (over z), fs: 4 (over y), tp: 8 (over x, core).
Axes of the slice: x: 4, y: 4, z: 4, core: 2. Of those that a mesh axis runs over, the one named last changes fastest.
Arguments:
- tokens_in: bfloat16 [12288, 1024], P(('rep', 'fs', 'tp')), may hold values from -6 to 6
- out_grad: bfloat16 [12288, 1024], P(('rep', 'fs', 'tp')), may hold values from -24 to 24
- gate_weight: bfloat16 [1024, 2816], P('fs', 'tp'), may hold values from -0.1875 to 0.1875
- up_weight: bfloat16 [1024, 2816], P('fs', 'tp'), may hold values from -0.1875 to 0.1875
- down_weight: bfloat16 [2816, 1024], P('tp', 'fs'), may hold values from -0.109375 to 0.109375
Outputs:
- grad_in: bfloat16 [12288, 1024], P(('rep', 'fs', 'tp'))
- grad_gate_w: float32 [1024, 2816], P('fs', 'tp')
- grad_up_w: float32 [1024, 2816], P('fs', 'tp')
- grad_down_w: float32 [2816, 1024], P('tp', 'fs')
All inputs are finite; a program needn't handle non-finite values.
Results may differ from a plain program's by a relative error of at most 0.02.
Values may be sent and summed in bfloat16 or wider, within the bound.
A program may use at most 64 MiB of HBM per device.

v0:
```python
import jax
import jax.numpy as jnp
from jax import lax
from jax.sharding import PartitionSpec as P


def summed_rows(product, width, axis):
    everything = product(jnp.int32(0), lax.axis_size(axis) * width)
    own = lax.psum_scatter(everything.astype(jnp.bfloat16), axis, scatter_dimension=0, tiled=True)
    return own.astype(jnp.float32)


def padded_to(lines, peers):
    spare = -len(lines) % peers
    return jnp.pad(lines, [(0, spare)] + [(0, 0)] * (lines.ndim - 1))


def total_of(x, axis):
    lines = x.reshape(-1, *x.shape[1:][-1:])
    own = lax.psum_scatter(
        padded_to(lines, lax.axis_size(axis)), axis, scatter_dimension=0, tiled=True
    )
    whole = lax.all_gather(own, axis).reshape(-1, *lines.shape[1:])
    return lax.slice_in_dim(whole, 0, len(lines)).reshape(x.shape)


def contract_last(left, right):
    return lax.dot_general(
        left, right, (((1,), (1,)), ((), ())), preferred_element_type=jnp.float32
    )


def contract_first(left, right):
    return lax.dot_general(
        left, right, (((0,), (0,)), ((), ())), preferred_element_type=jnp.float32
    )


def body(tokens_in, out_grad, gate_weight, up_weight, down_weight):
    replicas = lax.axis_size("rep")
    shards = lax.axis_size("fs")
    columns = lax.axis_size("tp")
    local_rows = tokens_in.shape[0]
    model_width = gate_weight.shape[0] * shards
    hidden_cols = gate_weight.shape[1]
    factor = (local_rows * replicas * shards * columns) ** (-0.5)
    gate_full, up_full, down_full = (
        lax.all_gather(gate_weight, "fs", axis=0, tiled=True),
        lax.all_gather(up_weight, "fs", axis=0, tiled=True),
        lax.all_gather(down_weight, "fs", axis=1, tiled=True),
    )
    tokens_all, grads_all = (
        lax.all_gather(tokens_in, "tp", axis=0, tiled=True),
        lax.all_gather(out_grad, "tp", axis=0, tiled=True),
    )
    gate = jnp.dot(tokens_all, gate_full, preferred_element_type=jnp.float32).astype(jnp.bfloat16)
    up_proj = jnp.dot(tokens_all, up_full, preferred_element_type=jnp.float32).astype(jnp.bfloat16)
    gate_wide = gate.astype(jnp.float32)
    up_wide = up_proj.astype(jnp.float32)
    sigmoid = jax.nn.sigmoid(gate_wide)
    activated = gate_wide * sigmoid
    hidden = (activated * up_wide).astype(jnp.bfloat16)
    grad_hidden = contract_last(grads_all, down_full).astype(jnp.bfloat16)
    grad_wide = grad_hidden.astype(jnp.float32)
    grad_gate = (grad_wide * up_wide * sigmoid * (1.0 + gate_wide * (1.0 - sigmoid))).astype(
        jnp.bfloat16
    )
    grad_up = (grad_wide * activated).astype(jnp.bfloat16)

    def input_term(start, count):
        gate_rows = lax.dynamic_slice_in_dim(grad_gate, start, count, 0)
        up_rows = lax.dynamic_slice_in_dim(grad_up, start, count, 0)
        return contract_last(gate_rows, gate_full) + contract_last(up_rows, up_full)

    grad_in = summed_rows(input_term, local_rows, "tp").astype(jnp.bfloat16)

    def weight_term(token_order, grad_order):

        def term(start, count):
            token_cols = lax.dynamic_slice_in_dim(token_order, start, count, 1)
            grad_cols = lax.dynamic_slice_in_dim(grad_order, start, count, 1)
            return factor * jnp.concatenate(
                [
                    contract_first(token_cols, grad_gate),
                    contract_first(token_cols, grad_up),
                    contract_first(grad_cols, hidden),
                ],
                axis=1,
            )

        return term

    owned = summed_rows(weight_term(tokens_all, grads_all), model_width // shards, "fs")
    summed = total_of(owned.astype(jnp.bfloat16), "rep").astype(jnp.float32)
    grad_gate_w = summed[:, :hidden_cols]
    grad_up_w = summed[:, hidden_cols : 2 * hidden_cols]
    grad_down_w = summed[:, 2 * hidden_cols :].T
    return (grad_in, grad_gate_w, grad_up_w, grad_down_w)


def solution(mesh):
    return jax.shard_map(
        body,
        mesh=mesh,
        in_specs=(
            P(("rep", "fs", "tp"), None),
            P(("rep", "fs", "tp"), None),
            P("fs", "tp"),
            P("fs", "tp"),
            P("tp", "fs"),
        ),
        out_specs=(P(("rep", "fs", "tp"), None), P("fs", "tp"), P("fs", "tp"), P("tp", "fs")),
        check_vma=False,
    )
```

profile of v0, /device:TPU:0, one launch (start us, length us, event | category | flops | bytes accessed | tf_op | source)
XLA Modules:
  0.0 167.5 jit_solution(8725800605460358486)
XLA Ops:
  7.2 0.0 copy-start
  7.2 0.0 copy-start.1
  7.2 0.0 all-gather.6.cloned.1.call-start
  7.2 0.7 all-gather.6.cloned.1.call-update
  7.9 0.0 all-gather.4.cloned.1.call-start
  8.0 0.7 all-gather.4.cloned.1.call-update
  8.7 0.0 reduce-scatter.8.cloned.1.call-start
  8.7 14.1 %all_gather.25 = bf16[1024,352]{0,1:T(8,128)(2,1)S(1)} all-gather(bf16[256,352]{0,1:T(8,128)(2,1)} %param.7), channel_id=1, replica_groups=mesh['rep'=4,'fs'=4,'tp'=8] {'fs'}, dimensions={0}, use_global_device_ids=true | all-gather | bytes 901120 | tf_op jit(solution)/shard_map/all_gather | solution.py:48
  22.8 0.0 copy-done
  22.8 13.5 %all_gather.24 = bf16[1024,352]{0,1:T(8,128)(2,1)S(1)} all-gather(bf16[256,352]{0,1:T(8,128)(2,1)S(1)} %copy-done), channel_id=1, replica_groups=mesh['rep'=4,'fs'=4,'tp'=8] {'fs'}, dimensions={0}, use_global_device_ids=true | all-gather | bytes 901120 | tf_op jit(solution)/shard_map/all_gather | solution.py:49
  36.3 0.0 copy-done.1
  36.3 14.3 %all_gather.22 = bf16[352,1024]{1,0:T(8,128)(2,1)S(1)} all-gather(bf16[352,256]{1,0:T(8,128)(2,1)S(1)} %copy-done.1), channel_id=1, replica_groups=mesh['rep'=4,'fs'=4,'tp'=8] {'fs'}, dimensions={1}, use_global_device_ids=true | all-gather | bytes 901120 | tf_op jit(solution)/shard_map/all_gather | solution.py:50
  50.6 2.3 %convolution_convert_fusion = bf16[768,352]{0,1:T(8,128)(2,1)S(1)} fusion(bf16[768,1024]{1,0:T(8,128)(2,1)} %all-gather.6.cloned.1.call-done, bf16[1024,352]{0,1:T(8,128)(2,1)S(1)} %all_gather.25), kind=kOutput, calls=%fused_computation.12 | convolution fusion | flops 553918464 | bytes 2834432 | tf_op jit(solution)/shard_map/dot_general | solution.py:56
  52.9 0.0 copy-done.2
  52.9 1.6 convolution_convert_fusion.1
  54.5 8.4 %all-gather.4.cloned.1.call-done = bf16[768,1024]{1,0:T(8,128)(2,1)} async-done(((bf16[96,1024]{1,0:T(8,128)(2,1)}), bf16[768,1024]{1,0:T(8,128)(2,1)}) %all-gather.4.cloned.1.call-update) | async-done | bytes 1572880 | tf_op jit(solution)/shard_map/all_gather | solution.py:54
  62.8 2.3 %convolution_convert_fusion.2 = bf16[768,352]{0,1:T(8,128)(2,1)S(1)} fusion(bf16[768,1024]{1,0:T(8,128)(2,1)} %all-gather.4.cloned.1.call-done, bf16[352,1024]{1,0:T(8,128)(2,1)S(1)} %all_gather.22), kind=kOutput, calls=%fused_computation.14 | convolution fusion | flops 553918464 | bytes 2834432 | tf_op jit(solution)/shard_map/dot_general | solution.py:28
  65.2 0.0 copy-done.4
  65.2 0.0 copy-done.5
  65.2 0.0 copy-start.7
  65.2 0.0 copy-start.3
  65.2 0.8 convolution_bitcast_fusion
  66.0 0.8 copy-done.3
  66.8 1.0 convolution_bitcast_fusion.2
  67.8 0.0 copy-done.7
  67.8 0.8 convolution_bitcast_fusion.1
  68.7 2.0 %fusion = bf16[1024,1056]{0,1:T(8,128)(2,1)} fusion(f32[1024,352]{0,1:T(8,128)S(1)} %convolution_bitcast_fusion, f32[1024,352]{0,1:T(8,128)S(1)} %convolution_bitcast_fusion.1, f32[1024,352]{0,1:T(8,128)S(1)} %convolution_bitcast_fusion.2), kind=kLoop, calls=%fused_computation.1 | loop fusion | flops 4325376 | bytes 6488064 | tf_op jit(solution)/shard_map/convert_element_type | solution.py:9
  70.7 0.0 reduce-scatter.8.cloned.1.call-update
  70.7 0.0 copy-start.6
  70.7 0.0 reduce-scatter.10.cloned.1.call-start
  70.8 30.6 %reduce-scatter.8.cloned.1.call-done = bf16[256,1056]{0,1:T(8,128)(2,1)} async-done(((bf16[1024,1056]{0,1:T(8,128)(2,1)}), bf16[256,1056]{0,1:T(8,128)(2,1)}) %reduce-scatter.8.cloned.1.call-update) | async-done | bytes 540688 | tf_op jit(solution)/shard_map/reduce_scatter | solution.py:9
  101.3 2.1 %copy.13 = bf16[256,1056]{1,0:T(8,128)(2,1)} copy(bf16[256,1056]{0,1:T(8,128)(2,1)} %reduce-scatter.8.cloned.1.call-done) | data formatting | bytes 1081344
  103.5 0.0 reduce-scatter.10.cloned.1.call-update
  103.5 0.0 reduce-scatter.6.cloned.1.call-start
  103.5 0.0 copy-done.6
  103.5 0.0 copy-done.8
  103.6 1.3 fusion.15
  104.8 2.3 %add_convert_fusion = bf16[768,1024]{1,0:T(8,128)(2,1)} fusion(f32[768,1024]{1,0:T(8,128)S(1)} %fusion.15, bf16[1024,352]{0,1:T(8,128)(2,1)S(1)} %all_gather.24, bf16[768,352]{0,1:T(8,128)(2,1)S(1)} %copy-done.8, bf16[768,352]{0,1:T(8,128)(2,1)S(1)} %convolution_convert_fusion), kind=kOutput, calls=%fused_computation.2 | convolution fusion | flops 557383680 | bytes 6520832 | tf_op jit(solution)/shard_map/dot_general | solution.py:28
  107.2 0.0 reduce-scatter.6.cloned.1.call-update
  107.2 18.3 %reduce-scatter.10.cloned.1.call-done = bf16[64,1056]{1,0:T(8,128)(2,1)} async-done(((bf16[256,1056]{1,0:T(8,128)(2,1)}), bf16[64,1056]{1,0:T(8,128)(2,1)}) %reduce-scatter.10.cloned.1.call-update) | async-done | bytes 135184 | tf_op jit(solution)/shard_map/reduce_scatter | solution.py:20
  125.5 13.1 %all-gather = bf16[256,1056]{1,0:T(8,128)(2,1)S(1)} all-gather(bf16[64,1056]{1,0:T(8,128)(2,1)} %reduce-scatter.10.cloned.1.call-done), channel_id=2, replica_groups=mesh['rep'=4,'fs'=4,'tp'=8] {'rep'}, dimensions={0}, use_global_device_ids=true | all-gather | bytes 675840 | tf_op jit(solution)/shard_map/all_gather | solution.py:23
  138.6 0.1 convert_element_type.57
  138.7 0.1 fusion.17
  138.8 0.9 copy.11
  139.7 0.9 copy.10
  140.6 0.2 slice_bitcast_fusion
  140.8 0.9 copy.12
  141.7 19.3 %reduce-scatter.6.cloned.1.call-done = bf16[96,1024]{1,0:T(8,128)(2,1)} async-done(((bf16[768,1024]{1,0:T(8,128)(2,1)}), bf16[96,1024]{1,0:T(8,128)(2,1)}) %reduce-scatter.6.cloned.1.call-update) | async-done | bytes 196624 | tf_op jit(solution)/shard_map/reduce_scatter | solution.py:9
  (5 shorter events, 0.0 us)
Async XLA Ops:
  7.2 15.6 %copy-start = (bf16[256,352]{0,1:T(8,128)(2,1)S(1)}, bf16[256,352]{0,1:T(8,128)(2,1)}, u32[]{:S(2)}) copy-start(bf16[256,352]{0,1:T(8,128)(2,1)} %param.8) | copy-start | bytes 540676
  7.2 29.1 %copy-start.1 = (bf16[352,256]{1,0:T(8,128)(2,1)S(1)}, bf16[352,256]{1,0:T(8,128)(2,1)}, u32[]{:S(2)}) copy-start(bf16[352,256]{1,0:T(8,128)(2,1)} %param.9) | copy-start | bytes 540676
  7.2 43.4 %all-gather.6.cloned.1.call-start = ((), (), s32[]{:S(2)}) async-start(), calls=%async_computation.4 | async-start | bytes 1769472 | tf_op jit(solution)/shard_map/all_gather | solution.py:53
  7.9 54.9 %all-gather.4.cloned.1.call-start = ((), (), s32[]{:S(2)}) async-start(), calls=%async_computation.3 | async-start | bytes 1769472 | tf_op jit(solution)/shard_map/all_gather | solution.py:54
  8.7 92.7 %reduce-scatter.8.cloned.1.call-start = ((), (), s32[]{:S(2)}) async-start(), calls=%async_computation.6 | async-start | bytes 2703360 | tf_op jit(solution)/shard_map/reduce_scatter | solution.py:9
  50.6 2.3 %copy-start.2 = (bf16[768,1024]{1,0:T(8,128)(2,1)S(1)}, bf16[768,1024]{1,0:T(8,128)(2,1)}, u32[]{:S(2)}) copy-start(bf16[768,1024]{1,0:T(8,128)(2,1)} %all-gather.6.cloned.1.call-done) | copy-start | bytes 4718596
  62.8 2.3 %copy-start.4 = (bf16[768,1024]{1,0:T(8,128)(2,1)S(1)}, bf16[768,1024]{1,0:T(8,128)(2,1)}, u32[]{:S(2)}) copy-start(bf16[768,1024]{1,0:T(8,128)(2,1)} %all-gather.4.cloned.1.call-done) | copy-start | bytes 4718596
  62.8 2.3 %copy-start.5 = (bf16[768,352]{0,1:T(8,128)(2,1)S(1)}, bf16[768,352]{0,1:T(8,128)(2,1)}, u32[]{:S(2)}) copy-start(bf16[768,352]{0,1:T(8,128)(2,1)} %convolution_convert_fusion.1) | copy-start | bytes 1622020
  65.2 2.6 %copy-start.7 = (bf16[768,352]{0,1:T(8,128)(2,1)}, bf16[768,352]{0,1:T(8,128)(2,1)S(1)}, u32[]{:S(2)}) copy-start(bf16[768,352]{0,1:T(8,128)(2,1)S(1)} %convolution_convert_fusion.2) | copy-start | bytes 1622020
  65.2 1.6 copy-start.3
  70.7 32.8 %copy-start.6 = (bf16[768,352]{0,1:T(8,128)(2,1)S(1)}, bf16[768,352]{0,1:T(8,128)(2,1)}, u32[]{:S(2)}) copy-start(bf16[768,352]{0,1:T(8,128)(2,1)} %convolution_convert_fusion.1) | copy-start | bytes 1622020
  70.7 32.8 %copy-start.8 = (bf16[768,352]{0,1:T(8,128)(2,1)S(1)}, bf16[768,352]{0,1:T(8,128)(2,1)}, u32[]{:S(2)}) copy-start(bf16[768,352]{0,1:T(8,128)(2,1)} %copy-done.7) | copy-start | bytes 1622020
  70.7 54.8 %reduce-scatter.10.cloned.1.call-start = ((), (), s32[]{:S(2)}) async-start(), calls=%async_computation.7 | async-start | bytes 737280 | tf_op jit(solution)/shard_map/reduce_scatter | solution.py:20
  103.5 57.4 %reduce-scatter.6.cloned.1.call-start = ((), (), s32[]{:S(2)}) async-start(), calls=%async_computation.5 | async-start | bytes 1769472 | tf_op jit(solution)/shard_map/reduce_scatter | solution.py:9
Sparse Core Ops, SparseCore 0:
  9.7 26.8 all-gather.5
  38.2 24.5 all-gather.3
  70.8 30.4 reduce-scatter.7
  103.6 21.8 reduce-scatter.9
  128.3 32.5 reduce-scatter.5
where the time goes:
time: 168 us; the launch traced here: 167 us
  waiting for transfers between devices  77.9 us (46%)
  blocking collectives  55 us (33%)
  between operations  13.9 us (8%)
  matrix products  12.5 us (7%)
  local copies, waits for them, and re-layouts  5.9 us (4%)
  other arithmetic  2.08 us (1%)
    reduce_scatter x2, waiting for transfers between devices, summed_rows(): lax.psum_scatter(everything.astype(jnp.bfloat16), axis, scatter_dimension...  49.8 us
    reduce_scatter x1, waiting for transfers between devices, total_of(): lax.psum_scatter(padded_to(lines, lax.axis_size(axis)), axis, scatter_dim...  18.3 us
    all_gather x1, blocking collectives, body(): lax.all_gather(down_weight, 'fs', axis=1, tiled=True)  14.3 us
    all_gather x1, blocking collectives, body(): lax.all_gather(gate_weight, 'fs', axis=0, tiled=True)  14.1 us
    all_gather x1, blocking collectives, body(): lax.all_gather(up_weight, 'fs', axis=0, tiled=True)  13.5 us
    all_gather x1, blocking collectives, total_of(): whole = lax.all_gather(own, axis).reshape(-1, *lines.shape[1:])  13.1 us
    all_gather x1, waiting for transfers between devices, body(): lax.all_gather(out_grad, 'tp', axis=0, tiled=True)  8.36 us
    dot_general x3, matrix products, contract_last(): lax.dot_general(left, right, (((1,), (1,)), ((), ())), preferred_element_...  5.94 us
  transfers between devices with their start and end apart: 5, of which 4 were waited for; matrix products, arithmetic and copies ran while one was open for 6% of the time, Pallas kernels for 0%

commit v1 on v0

v1 whole, which is shorter than its diff:
```python
import functools

import jax
import jax.numpy as jnp
from jax import lax
from jax.experimental import pallas as pl
from jax.experimental.pallas import tpu as pltpu
from jax.sharding import PartitionSpec as P

BF16 = jnp.bfloat16
F32 = jnp.float32
MESH = pl.DeviceIdType.MESH
COPIES = 112


def nt(left, right):
    return lax.dot_general(left, right, (((1,), (1,)), ((), ())), preferred_element_type=F32)


def tn(left, right):
    return lax.dot_general(left, right, (((0,), (0,)), ((), ())), preferred_element_type=F32)


def nn(left, right):
    return lax.dot_general(left, right, (((1,), (0,)), ((), ())), preferred_element_type=F32)


def eye(n):
    rows = lax.broadcasted_iota(jnp.int32, (n, n), 0)
    cols = lax.broadcasted_iota(jnp.int32, (n, n), 1)
    return jnp.where(rows == cols, 1.0, 0.0).astype(BF16)


def kernel(
    factor, block, width, hid,
    x_in, g_in, wg_in, wu_in, wd_in,
    gin_out, og_out, ou_out, od_out,
    X, G, WT, WG, WU, H, PW, PB, DX, DS, GX, YA1, YA2, ZB, OUTT,
    ring_bufs,
    send_sems, recv_sems, local_sems,
):
    rep = lax.axis_index("rep")
    fs = lax.axis_index("fs")
    tp = lax.axis_index("tp")
    core = lax.rem(tp, 2)
    xpos = tp // 2
    shard = width // 4

    def turn(pos, step):
        return lax.rem(pos + step, 4)

    def at_x(step):
        return {"tp": turn(xpos, step) * 2 + core}

    def at_y(step):
        return {"fs": turn(fs, step)}

    def at_z(step):
        return {"rep": turn(rep, step)}

    sibling = {"tp": tp + 1 - 2 * core}

    def lanes_of(step):
        return pl.ds(pl.multiple_of(turn(fs, step) * shard, shard), shard)

    counter = [0]
    pending = []

    def remote(src, dst, k, where):
        return pltpu.make_async_remote_copy(
            src_ref=src, dst_ref=dst, send_sem=send_sems.at[k], recv_sem=recv_sems.at[k],
            device_id=where, device_id_type=MESH,
        )

    def send(src, dst, where):
        k = counter[0]
        counter[0] += 1
        copy = remote(src, dst, k, where)
        copy.start()
        pending.append(copy)
        return k

    def arrived(k, landing):
        remote(landing, landing, k, sibling).wait_recv()

    own_lanes = lanes_of(0)
    loads = [
        pltpu.make_async_copy(x_in, X.at[pl.ds(0, block)], local_sems.at[0]),
        pltpu.make_async_copy(g_in, G.at[pl.ds(0, block)], local_sems.at[1]),
        pltpu.make_async_copy(wg_in, WG, local_sems.at[2]),
        pltpu.make_async_copy(wu_in, WU, local_sems.at[3]),
        pltpu.make_async_copy(wd_in, WT.at[pl.ds(2 * hid, hid), own_lanes], local_sems.at[4]),
    ]
    for load in loads:
        load.start()

    barrier = pltpu.get_barrier_semaphore()
    for where in (at_x(1), at_x(3), at_y(1), at_y(3), at_z(1), at_z(3), sibling):
        pl.semaphore_signal(barrier, inc=1, device_id=where, device_id_type=MESH)
    pl.semaphore_wait(barrier, 7)

    half = block // 2
    SELF, LEFT, RIGHT, OPP = 0, 1, 2, 3

    def slot(buf, s, start=0, count=block):
        return buf.at[pl.ds(s * 2 * block + start, count)]

    def token_start(buf):
        right = send(slot(buf, SELF), slot(buf, LEFT), at_x(1))
        left = send(slot(buf, SELF), slot(buf, RIGHT), at_x(3))
        across = send(slot(buf, SELF), slot(buf, SELF, block), sibling)
        return right, left, [(across, SELF)]

    def token_relay(buf, state):
        right, left, across = state
        arrived(right, slot(buf, LEFT))
        right = send(slot(buf, LEFT, 0, half), slot(buf, OPP, 0, half), at_x(1))
        arrived(left, slot(buf, RIGHT))
        left = send(slot(buf, RIGHT, half, half), slot(buf, OPP, half, half), at_x(3))
        across.append((send(slot(buf, LEFT), slot(buf, LEFT, block), sibling), LEFT))
        across.append((send(slot(buf, RIGHT), slot(buf, RIGHT, block), sibling), RIGHT))
        return right, left, across

    def token_last(buf, state):
        right, left, across = state
        arrived(right, slot(buf, OPP, 0, half))
        arrived(left, slot(buf, OPP, half, half))
        return [(send(slot(buf, OPP), slot(buf, OPP, block), sibling), OPP)]

    def token_wait(buf, across):
        for k, s in across:
            arrived(k, slot(buf, s, block))

    loads[0].wait()
    x_state = token_start(X)
    loads[1].wait()
    g_state = token_start(G)

    identity = eye(hid)
    loads[3].wait()
    WT[pl.ds(hid, hid), own_lanes] = nt(identity, WU[...]).astype(BF16)
    loads[4].wait()
    loads[2].wait()
    WT[pl.ds(0, hid), own_lanes] = nt(identity, WG[...]).astype(BF16)

    direct = 544
    part = (3 * hid - direct) // 4
    dhalf = direct // 2
    D0, D1 = pl.ds(0, dhalf), pl.ds(dhalf, dhalf)

    def quarter(step, start=0, count=part):
        return pl.ds(pl.multiple_of(direct + turn(rep, step) * part + start, 16), count)

    def w(rows, step):
        return WT.at[rows, lanes_of(step)]

    qa = send(w(quarter(0), 0), w(quarter(0), 0), at_y(1))
    qb = send(w(quarter(0), 0), w(quarter(0), 0), at_y(3))
    d0r = send(w(D0, 0), w(D0, 0), at_y(1))
    d1l = send(w(D1, 0), w(D1, 0), at_y(3))

    qh = part // 2
    arrived(qa, w(quarter(0), 3))
    qc = send(w(quarter(0, 0, qh), 3), w(quarter(0, 0, qh), 3), at_y(1))
    arrived(qb, w(quarter(0), 1))
    qd = send(w(quarter(0, qh, qh), 1), w(quarter(0, qh, qh), 1), at_y(3))
    d1r = send(w(D1, 0), w(D1, 0), at_y(1))
    d0l = send(w(D0, 0), w(D0, 0), at_y(3))

    def share(step):
        return (
            send(w(quarter(0), step), w(quarter(0), step), at_z(1)),
            send(w(quarter(0), step), w(quarter(0), step), at_z(3)),
        )

    def share_relay(state, step):
        arrived(state[0], w(quarter(3), step))
        a = send(w(quarter(3, 0, qh), step), w(quarter(3, 0, qh), step), at_z(1))
        arrived(state[1], w(quarter(1), step))
        b = send(w(quarter(1, qh, qh), step), w(quarter(1, qh, qh), step), at_z(3))
        return a, b

    def share_last(state, step):
        arrived(state[0], w(quarter(2, 0, qh), step))
        arrived(state[1], w(quarter(2, qh, qh), step))

    z3 = share(3)
    z1 = share(1)

    x_state = token_relay(X, x_state)

    arrived(d0r, w(D0, 3))
    dc = send(w(D0, 3), w(D0, 3), at_y(1))
    arrived(d1l, w(D1, 1))
    dd = send(w(D1, 1), w(D1, 1), at_y(3))

    z3 = share_relay(z3, 3)
    arrived(qc, w(quarter(0, 0, qh), 2))
    arrived(qd, w(quarter(0, qh, qh), 2))
    z2 = share(2)
    z1 = share_relay(z1, 1)

    z2 = share_relay(z2, 2)
    g_state = token_relay(G, g_state)
    x_last = token_last(X, x_state)

    arrived(d1r, w(D1, 3))
    arrived(d0l, w(D0, 1))
    for state, step in ((z3, 3), (z1, 1), (z2, 2)):
        share_last(state, step)
    arrived(dc, w(D0, 2))
    arrived(dd, w(D1, 2))

    rows = hid // 2

    def first_stage(c):
        cols = pl.ds(c * 256, 256)
        for p in range(2):
            gate = nt(WT[pl.ds(p * rows, rows), :], X[cols, :]).astype(BF16).astype(F32)
            up = nt(WT[pl.ds(hid + p * rows, rows), :], X[cols, :]).astype(BF16).astype(F32)
            grad = nt(WT[pl.ds(2 * hid + p * rows, rows), :], G[cols, :]).astype(BF16).astype(F32)
            sig = jax.nn.sigmoid(gate)
            act = gate * sig
            H[pl.ds(2 * hid + p * rows, rows), cols] = (act * up).astype(BF16)
            H[pl.ds(p * rows, rows), cols] = (
                grad * up * sig * (1.0 + gate * (1.0 - sig))
            ).astype(BF16)
            H[pl.ds(hid + p * rows, rows), cols] = (grad * act).astype(BF16)

    token_wait(X, x_state[2])
    token_wait(G, g_state[2])
    first_stage(0)
    g_last = token_last(G, g_state)
    first_stage(1)
    token_wait(X, x_last)
    token_wait(G, g_last)
    first_stage(2)

    class Ring:
        def __init__(self, piece, bufs, dest):
            self.piece, self.dest = piece, dest
            self.t0, self.t1, self.fl, self.fr = bufs
            self.h = self.t0.shape[1]

        def side(self, buf, which):
            return buf.at[:, pl.ds(which * self.h, self.h)]

        def start_far(self):
            self.a = send(self.piece(2, 0), self.t0, self.dest(1))
            self.b = send(self.piece(2, 1), self.t1, self.dest(3))

        def start_near(self):
            self.c = send(self.piece(1, 1), self.side(self.fl, 1), self.dest(1))
            self.d = send(self.piece(3, 0), self.side(self.fr, 0), self.dest(3))

        def relay(self):
            arrived(self.a, self.t0)
            self.t0[...] = (self.t0[...].astype(F32) + self.piece(1, 0)[...].astype(F32)).astype(BF16)
            self.e = send(self.t0, self.side(self.fl, 0), self.dest(1))
            arrived(self.b, self.t1)
            self.t1[...] = (self.t1[...].astype(F32) + self.piece(3, 1)[...].astype(F32)).astype(BF16)
            self.f = send(self.t1, self.side(self.fr, 1), self.dest(3))

        def finish(self, store):
            arrived(self.c, self.side(self.fl, 1))
            arrived(self.d, self.side(self.fr, 0))
            arrived(self.e, self.side(self.fl, 0))
            arrived(self.f, self.side(self.fr, 1))
            for which in range(2):
                total = (
                    self.piece(0, which)[...].astype(F32)
                    + self.side(self.fl, which)[...].astype(F32)
                    + self.side(self.fr, which)[...].astype(F32)
                )
                store(which, total.astype(BF16))

    def y_piece(buf, start, count):
        def piece(step, which):
            lane = pl.multiple_of(turn(fs, step) * shard + which * (shard // 2), 128)
            return buf.at[pl.ds(start, count), pl.ds(lane, shard // 2)]
        return piece

    def z_piece(buf, count, lanes):
        def piece(step, which):
            row = pl.multiple_of(turn(rep, step) * count, 16)
            return buf.at[pl.ds(row, count), pl.ds(which * lanes, lanes)]
        return piece

    def x_piece(step, which):
        s = {0: SELF, 1: RIGHT, 3: LEFT, 2: OPP}[step]
        return GX.at[pl.ds(s * block, block), pl.ds(which * (width // 2), width // 2)]

    A1, A2 = 384, 2 * hid - 384
    B = PB.shape[0]
    ya1 = Ring(y_piece(PW, 0, A1), ring_bufs[0:4], at_y)
    ya2 = Ring(y_piece(PW, A1, A2), ring_bufs[4:8], at_y)
    zb = Ring(z_piece(PB, B // 4, width // 2), ring_bufs[8:12], at_z)
    za1 = Ring(z_piece(YA1, A1 // 4, shard // 2), ring_bufs[12:16], at_z)
    za2 = Ring(z_piece(YA2, A2 // 4, shard // 2), ring_bufs[16:20], at_z)
    yb = Ring(y_piece(ZB, 0, B // 4), ring_bufs[20:24], at_y)
    xr = Ring(x_piece, ring_bufs[24:28], at_x)

    def to_rows(buf, start):
        def store(which, value):
            n, h = value.shape
            buf[pl.ds(start, n), pl.ds(which * h, h)] = value
        return store

    class Gather:
        def __init__(self, base, count):
            self.base, self.count = base, count

        def row(self, step):
            return pl.multiple_of(self.base + turn(rep, step) * self.count, 16)

        def region(self, step, which=None):
            if which is None:
                return OUTT.at[pl.ds(self.row(step), self.count)]
            return OUTT.at[pl.ds(self.row(step), self.count), pl.ds(which * (shard // 2), shard // 2)]

        def start(self):
            self.a = send(self.region(0), self.region(0), at_z(1))
            self.b = send(self.region(0), self.region(0), at_z(3))

        def relay(self):
            arrived(self.a, self.region(3))
            self.c = send(self.region(3, 0), self.region(3, 0), at_z(1))
            arrived(self.b, self.region(1))
            self.d = send(self.region(1, 1), self.region(1, 1), at_z(3))

        def finish(self):
            arrived(self.c, self.region(2, 0))
            arrived(self.d, self.region(2, 1))

    ga1, ga2, gb = Gather(0, A1 // 4), Gather(A1, A2 // 4), Gather(2 * hid, B // 4)

    def weight_piece(step, start, count):
        lanes = lanes_of(step)
        PW[pl.ds(start, count), lanes] = (
            factor * nn(H[pl.ds(start, count), :], X[:, lanes])
        ).astype(BF16)

    def input_piece(c):
        DX[pl.ds(c * 256, 256), :] = tn(
            H[pl.ds(0, 2 * hid), pl.ds(c * 256, 256)], WT[pl.ds(0, 2 * hid), :]
        ).astype(BF16)

    def across(s):
        landing = DS.at[pl.ds(s * block, block)]
        return send(slot(DX, s, block), landing, sibling)

    def across_add(k, s):
        arrived(k, DS.at[pl.ds(s * block, block)])
        GX[pl.ds(s * block, block), :] = (
            DX[pl.ds(s * 2 * block, block), :].astype(F32)
            + DS[pl.ds(s * block, block), :].astype(F32)
        ).astype(BF16)

    weight_piece(2, 0, A1)
    ya1.start_far()
    PB[pl.ds(hid, B - hid), :] = jnp.zeros((B - hid, width), BF16)
    for n in range(4):
        PB[pl.ds(0, hid), pl.ds(n * 256, 256)] = (
            factor * nn(H[pl.ds(2 * hid, hid), :], G[:, pl.ds(n * 256, 256)])
        ).astype(BF16)
    zb.start_far()
    zb.start_near()
    weight_piece(1, 0, A1)
    weight_piece(3, 0, A1)
    ya1.start_near()
    input_piece(2)
    opp = across(OPP)
    for step in (2, 1, 3, 0):
        weight_piece(step, A1, A2)
    ya1.relay()
    ya2.start_far()
    ya2.start_near()
    zb.relay()
    weight_piece(0, 0, A1)
    across_add(opp, OPP)
    xr.start_far()
    input_piece(1)
    near = across(LEFT), across(RIGHT)
    input_piece(0)
    mine = across(SELF)
    across_add(near[0], LEFT)
    across_add(near[1], RIGHT)
    xr.start_near()
    ya1.finish(to_rows(YA1, 0))
    za1.start_far()
    za1.start_near()

    def zb_store(which, value):
        ZB[:, pl.ds(which * (width // 2), width // 2)] = value

    zb.finish(zb_store)
    ya2.relay()
    yb.start_far()
    yb.start_near()
    xr.relay()
    across_add(mine, SELF)
    za1.relay()
    za1.finish(to_rows(OUTT, ga1.row(0)))
    ga1.start()
    yb.relay()
    ya2.finish(to_rows(YA2, 0))
    za2.start_far()
    za2.start_near()
    yb.finish(to_rows(OUTT, gb.row(0)))
    gb.start()
    ga1.relay()
    za2.relay()

    def gin_store(which, value):
        gin_out[:, pl.ds(which * (width // 2), width // 2)] = value

    xr.finish(gin_store)
    za2.finish(to_rows(OUTT, ga2.row(0)))
    ga2.start()
    gb.relay()
    ga1.finish()
    turned = eye(shard)
    gb.finish()
    od_out[...] = OUTT[pl.ds(2 * hid, hid), :].astype(F32)
    ga2.relay()
    og_out[...] = nt(turned, OUTT[pl.ds(0, hid), :])
    ga2.finish()
    ou_out[...] = nt(turned, OUTT[pl.ds(hid, hid), :])

    for copy in pending:
        copy.wait_send()


def body(tokens_in, out_grad, gate_weight, up_weight, down_weight):
    block, width = tokens_in.shape
    shard, hid = gate_weight.shape
    devices = lax.axis_size("rep") * lax.axis_size("fs") * lax.axis_size("tp")
    factor = (block * devices) ** (-0.5)
    tokens = block * 8
    A1, A2, B = 384, 2 * hid - 384, 384

    def ring(count, lanes):
        return [
            pltpu.VMEM((count, lanes // 2), BF16),
            pltpu.VMEM((count, lanes // 2), BF16),
            pltpu.VMEM((count, lanes), BF16),
            pltpu.VMEM((count, lanes), BF16),
        ]

    rings = (
        ring(A1, shard) + ring(A2, shard) + ring(B // 4, width)
        + ring(A1 // 4, shard) + ring(A2 // 4, shard) + ring(B // 4, shard)
        + ring(block, width)
    )
    return pl.pallas_call(
        functools.partial(kernel, factor, block, width, hid),
        out_shape=(
            jax.ShapeDtypeStruct((block, width), BF16),
            jax.ShapeDtypeStruct((shard, hid), F32),
            jax.ShapeDtypeStruct((shard, hid), F32),
            jax.ShapeDtypeStruct((hid, shard), F32),
        ),
        in_specs=[pl.BlockSpec(memory_space=pl.ANY)] * 5,
        out_specs=[pl.BlockSpec(memory_space=pltpu.VMEM)] * 4,
        scratch_shapes=[
            pltpu.VMEM((tokens, width), BF16),
            pltpu.VMEM((tokens, width), BF16),
            pltpu.VMEM((3 * hid, width), BF16),
            pltpu.VMEM((shard, hid), BF16),
            pltpu.VMEM((shard, hid), BF16),
            pltpu.VMEM((3 * hid, tokens), BF16),
            pltpu.VMEM((2 * hid, width), BF16),
            pltpu.VMEM((B, width), BF16),
            pltpu.VMEM((tokens, width), BF16),
            pltpu.VMEM((tokens // 2, width), BF16),
            pltpu.VMEM((tokens // 2, width), BF16),
            pltpu.VMEM((A1, shard), BF16),
            pltpu.VMEM((A2, shard), BF16),
            pltpu.VMEM((B // 4, width), BF16),
            pltpu.VMEM((2 * hid + B, shard), BF16),
            rings,
            pltpu.SemaphoreType.DMA((COPIES,)),
            pltpu.SemaphoreType.DMA((COPIES,)),
            pltpu.SemaphoreType.DMA((5,)),
        ],
        compiler_params=pltpu.CompilerParams(
            collective_id=0, has_side_effects=True, vmem_limit_bytes=48 * 1024 * 1024
        ),
    )(tokens_in, out_grad, gate_weight, up_weight, down_weight)


def solution(mesh):
    return jax.shard_map(
        body,
        mesh=mesh,
        in_specs=(
            P(("rep", "fs", "tp"), None),
            P(("rep", "fs", "tp"), None),
            P("fs", "tp"),
            P("fs", "tp"),
            P("tp", "fs"),
        ),
        out_specs=(P(("rep", "fs", "tp"), None), P("fs", "tp"), P("fs", "tp"), P("tp", "fs")),
        check_vma=False,
    )
```

time: 168 us -> 70.1 us (0.42)
  waiting for transfers between devices: 77.9 us -> 0 us
  Pallas kernels: 0 us -> 63.9 us
  blocking collectives: 55 us -> 0 us
  between operations: 13.9 us -> 0.7 us
  matrix products: 12.5 us -> 0 us
  other arithmetic: 2.08 us -> 0 us
    reduce_scatter x3 -> x0, waiting for transfers between devices: 68.1 us -> none  [the longest x2 49.8 us: summed_rows(): lax.psum_scatter(everything.astype(jnp.bfloat16), axis, scatter_dimension...]
    pallas_call x0 -> x1, Pallas kernels: none -> 63.9 us  [body(): pl.pallas_call(functools.partial(kernel, factor, block, width, hid), out_...]
    all_gather x4 -> x0, blocking collectives: 55 us -> none  [the longest x1 14.3 us: body(): lax.all_gather(down_weight, 'fs', axis=1, tiled=True)]
    dot_general x8 -> x0, matrix products: 12.5 us -> none  [the longest x3 5.94 us: contract_last(): lax.dot_general(left, right, (((1,), (1,)), ((), ())), preferred_element_...]
    all_gather x2 -> x0, waiting for transfers between devices: 8.37 us -> none  [the longest x1 8.36 us: body(): lax.all_gather(out_grad, 'tp', axis=0, tiled=True)]
    convert_element_type x2 -> x0, other arithmetic: 2.08 us -> none  [the longest x1 2.01 us: summed_rows(): everything.astype(jnp.bfloat16)]
    unnamed x22 -> x12, local copies, waits for them, and re-layouts: 5.62 us -> 3.54 us
    pallas_call x0 -> x2, local copies, waits for them, and re-layouts: none -> 1.79 us  [body(): pl.pallas_call(functools.partial(kernel, factor, block, width, hid), out_...]
  transfers between devices with their start and end apart: 5 -> 0, of which waited for: 4 -> 0; matrix products, arithmetic and copies ran while one was open for 6% -> 0% of each run, Pallas kernels for 0% -> 0%
where the time goes in v1:
time: 70.1 us; the launch traced here: 70 us
  Pallas kernels  63.9 us (91%)
  local copies, waits for them, and re-layouts  5.33 us (8%)
    pallas_call x1, Pallas kernels, body(): pl.pallas_call(functools.partial(kernel, factor, block, width, hid), out_...  63.9 us
    unnamed x12, local copies, waits for them, and re-layouts  3.54 us
    pallas_call x2, local copies, waits for them, and re-layouts, body(): pl.pallas_call(functools.partial(kernel, factor, block, width, hid), out_...  1.79 us

profile of v1, /device:TPU:0, one launch (start us, length us, event | category | flops | bytes accessed | tf_op | source)
XLA Modules:
  0.0 70.0 jit_solution(6331688158846946633)
XLA Ops:
  0.6 0.0 copy-start.3
  0.6 0.0 copy-start.1
  0.7 1.1 %copy.9.wg_in = bf16[256,352]{1,0:T(8,128)(2,1)S(1)} copy(bf16[256,352]{0,1:T(8,128)(2,1)} %param.7) | data formatting | bytes 360448 | tf_op args[2]
  1.8 0.0 copy-done.3
  1.8 0.0 copy-start
  1.8 0.0 copy-start.2
  1.8 0.2 copy.10.wu_in
  2.0 0.0 copy-done.1
  2.0 0.7 %copy-done = bf16[96,1024]{1,0:T(8,128)(2,1)S(1)} copy-done((bf16[96,1024]{1,0:T(8,128)(2,1)S(1)}, bf16[96,1024]{1,0:T(8,128)(2,1)}, u32[]{:S(2)}) %copy-start) | copy-done | bytes 196632
  2.7 0.1 copy-done.2
  2.8 63.9 %shard_map.84 = (bf16[96,1024]{1,0:T(8,128)(2,1)S(1)}, f32[256,352]{1,0:T(8,128)S(1)}, f32[256,352]{1,0:T(8,128)S(1)}, f32[352,256]{1,0:T(8,128)S(1)}) custom-call(bf16[96,1024]{1,0:T(8,128)(2,1)S(1)} %copy-done, bf16[96,1024]{1,0:T(8,128)(2,1)S(1)} %copy-done.1, bf16[256,352]{1,0:T(8,128)(2,1)S(1)} %copy.9.wg_in, bf16[256,352]{1,0:T(8,128)(2,1)S(1)} %copy.10.wu_in, ...), custom_call_target="tpu_custom_call" | custom-call | tf_op jit(solution)/shard_map/pallas_call | solution.py:455
  66.8 0.9 %copy.11 = f32[256,352]{0,1:T(8,128)} copy(f32[256,352]{1,0:T(8,128)S(1)} %get-tuple-element.5) | data formatting | bytes 720896 | tf_op jit(solution)/shard_map/pallas_call | solution.py:455
  67.7 0.9 %copy.12 = f32[256,352]{0,1:T(8,128)} copy(f32[256,352]{1,0:T(8,128)S(1)} %get-tuple-element.6) | data formatting | bytes 720896 | tf_op jit(solution)/shard_map/pallas_call | solution.py:455
  68.5 0.7 copy.15
  69.2 0.7 %copy.16 = f32[352,256]{1,0:T(8,128)} copy(f32[352,256]{1,0:T(8,128)S(1)} %get-tuple-element.15) | data formatting | bytes 720896
Async XLA Ops:
  0.6 1.2 %copy-start.3 = (bf16[256,352]{0,1:T(8,128)(2,1)S(1)}, bf16[256,352]{0,1:T(8,128)(2,1)}, u32[]{:S(2)}) copy-start(bf16[256,352]{0,1:T(8,128)(2,1)} %param.8) | copy-start | bytes 540676
  0.6 1.3 %copy-start.1 = (bf16[96,1024]{1,0:T(8,128)(2,1)S(1)}, bf16[96,1024]{1,0:T(8,128)(2,1)}, u32[]{:S(2)}) copy-start(bf16[96,1024]{1,0:T(8,128)(2,1)} %g_in.1) | copy-start | bytes 589828
  1.8 0.9 %copy-start = (bf16[96,1024]{1,0:T(8,128)(2,1)S(1)}, bf16[96,1024]{1,0:T(8,128)(2,1)}, u32[]{:S(2)}) copy-start(bf16[96,1024]{1,0:T(8,128)(2,1)} %x_in.1) | copy-start | bytes 589828
  1.8 1.0 %copy-start.2 = (bf16[352,256]{1,0:T(8,128)(2,1)S(1)}, bf16[352,256]{1,0:T(8,128)(2,1)}, u32[]{:S(2)}) copy-start(bf16[352,256]{1,0:T(8,128)(2,1)} %wd_in.1) | copy-start | bytes 540676

commit v2 on v1

--- a/solution.py
+++ b/solution.py
@@ -10,7 +10,8 @@
 BF16 = jnp.bfloat16
 F32 = jnp.float32
 MESH = pl.DeviceIdType.MESH
-COPIES = 112
+COPIES = 128
+SPLIT = (320, 256), (256, 256)
 
 
 def nt(left, right):
@@ -23,19 +24,13 @@
 
 def nn(left, right):
     return lax.dot_general(left, right, (((1,), (0,)), ((), ())), preferred_element_type=F32)
-
-
-def eye(n):
-    rows = lax.broadcasted_iota(jnp.int32, (n, n), 0)
-    cols = lax.broadcasted_iota(jnp.int32, (n, n), 1)
-    return jnp.where(rows == cols, 1.0, 0.0).astype(BF16)
 
 
 def kernel(
     factor, block, width, hid,
     x_in, g_in, wg_in, wu_in, wd_in,
     gin_out, og_out, ou_out, od_out,
-    X, G, WT, WG, WU, H, PW, PB, DX, DS, GX, YA1, YA2, ZB, OUTT,
+    X, G, WT, H, ACT, SLOPE, PW, DX, DS, GX, YA1, YA2, ZB1, ZB2, OUTT,
     ring_bufs,
     send_sems, recv_sems, local_sems,
 ):
@@ -87,8 +82,8 @@
     loads = [
         pltpu.make_async_copy(x_in, X.at[pl.ds(0, block)], local_sems.at[0]),
         pltpu.make_async_copy(g_in, G.at[pl.ds(0, block)], local_sems.at[1]),
-        pltpu.make_async_copy(wg_in, WG, local_sems.at[2]),
-        pltpu.make_async_copy(wu_in, WU, local_sems.at[3]),
+        pltpu.make_async_copy(wg_in, WT.at[pl.ds(0, hid), own_lanes], local_sems.at[2]),
+        pltpu.make_async_copy(wu_in, WT.at[pl.ds(hid, hid), own_lanes], local_sems.at[3]),
         pltpu.make_async_copy(wd_in, WT.at[pl.ds(2 * hid, hid), own_lanes], local_sems.at[4]),
     ]
     for load in loads:
@@ -109,7 +104,7 @@
         right = send(slot(buf, SELF), slot(buf, LEFT), at_x(1))
         left = send(slot(buf, SELF), slot(buf, RIGHT), at_x(3))
         across = send(slot(buf, SELF), slot(buf, SELF, block), sibling)
-        return right, left, [(across, SELF)]
+        return right, left, [(across, (SELF, block))]
 
     def token_relay(buf, state):
         right, left, across = state
@@ -117,31 +112,29 @@
         right = send(slot(buf, LEFT, 0, half), slot(buf, OPP, 0, half), at_x(1))
         arrived(left, slot(buf, RIGHT))
         left = send(slot(buf, RIGHT, half, half), slot(buf, OPP, half, half), at_x(3))
-        across.append((send(slot(buf, LEFT), slot(buf, LEFT, block), sibling), LEFT))
-        across.append((send(slot(buf, RIGHT), slot(buf, RIGHT, block), sibling), RIGHT))
+        across.append((send(slot(buf, LEFT), slot(buf, LEFT, block), sibling), (LEFT, block)))
+        across.append((send(slot(buf, RIGHT), slot(buf, RIGHT, block), sibling), (RIGHT, block)))
         return right, left, across
 
     def token_last(buf, state):
-        right, left, across = state
-        arrived(right, slot(buf, OPP, 0, half))
-        arrived(left, slot(buf, OPP, half, half))
-        return [(send(slot(buf, OPP), slot(buf, OPP, block), sibling), OPP)]
+        out = []
+        for k, start in ((state[0], 0), (state[1], half)):
+            arrived(k, slot(buf, OPP, start, half))
+            landing = (OPP, block + start, half)
+            out.append((send(slot(buf, OPP, start, half), slot(buf, *landing), sibling), landing))
+        return out
 
     def token_wait(buf, across):
-        for k, s in across:
-            arrived(k, slot(buf, s, block))
+        for k, landing in across:
+            arrived(k, slot(buf, *landing))
 
     loads[0].wait()
     x_state = token_start(X)
     loads[1].wait()
     g_state = token_start(G)
 
-    identity = eye(hid)
-    loads[3].wait()
-    WT[pl.ds(hid, hid), own_lanes] = nt(identity, WU[...]).astype(BF16)
-    loads[4].wait()
-    loads[2].wait()
-    WT[pl.ds(0, hid), own_lanes] = nt(identity, WG[...]).astype(BF16)
+    for load in loads[2:]:
+        load.wait()
 
     direct = 544
     part = (3 * hid - direct) // 4
@@ -200,10 +193,13 @@
     z2 = share(2)
     z1 = share_relay(z1, 1)
 
-    z2 = share_relay(z2, 2)
     g_state = token_relay(G, g_state)
     x_last = token_last(X, x_state)
-
+    z2 = share_relay(z2, 2)
+
+    token_wait(X, x_state[2])
+    token_wait(X, x_last)
+    token_wait(G, g_state[2])
     arrived(d1r, w(D1, 3))
     arrived(d0l, w(D0, 1))
     for state, step in ((z3, 3), (z1, 1), (z2, 2)):
@@ -213,28 +209,32 @@
 
     rows = hid // 2
 
-    def first_stage(c):
+    def gate_stage(c):
         cols = pl.ds(c * 256, 256)
         for p in range(2):
-            gate = nt(WT[pl.ds(p * rows, rows), :], X[cols, :]).astype(BF16).astype(F32)
+            part_rows = pl.ds(p * rows, rows)
+            gate = nt(WT[part_rows, :], X[cols, :]).astype(BF16).astype(F32)
             up = nt(WT[pl.ds(hid + p * rows, rows), :], X[cols, :]).astype(BF16).astype(F32)
-            grad = nt(WT[pl.ds(2 * hid + p * rows, rows), :], G[cols, :]).astype(BF16).astype(F32)
             sig = jax.nn.sigmoid(gate)
             act = gate * sig
             H[pl.ds(2 * hid + p * rows, rows), cols] = (act * up).astype(BF16)
-            H[pl.ds(p * rows, rows), cols] = (
-                grad * up * sig * (1.0 + gate * (1.0 - sig))
-            ).astype(BF16)
-            H[pl.ds(hid + p * rows, rows), cols] = (grad * act).astype(BF16)
-
-    token_wait(X, x_state[2])
-    token_wait(G, g_state[2])
-    first_stage(0)
+            ACT[part_rows, cols] = act
+            SLOPE[part_rows, cols] = up * sig * (1.0 + gate * (1.0 - sig))
+
+    def grad_stage(c):
+        cols = pl.ds(c * 256, 256)
+        grad = nt(WT[pl.ds(2 * hid, hid), :], G[cols, :]).astype(BF16).astype(F32)
+        H[pl.ds(0, hid), cols] = (grad * SLOPE[:, cols]).astype(BF16)
+        H[pl.ds(hid, hid), cols] = (grad * ACT[:, cols]).astype(BF16)
+
+    gate_stage(0)
+    gate_stage(1)
     g_last = token_last(G, g_state)
-    first_stage(1)
-    token_wait(X, x_last)
+    gate_stage(2)
+    grad_stage(0)
+    grad_stage(1)
     token_wait(G, g_last)
-    first_stage(2)
+    grad_stage(2)
 
     class Ring:
         def __init__(self, piece, bufs, dest):
@@ -280,9 +280,9 @@
             return buf.at[pl.ds(start, count), pl.ds(lane, shard // 2)]
         return piece
 
-    def z_piece(buf, count, lanes):
+    def z_piece(buf, start, count, lanes):
         def piece(step, which):
-            row = pl.multiple_of(turn(rep, step) * count, 16)
+            row = pl.multiple_of(start + turn(rep, step) * count, 16)
             return buf.at[pl.ds(row, count), pl.ds(which * lanes, lanes)]
         return piece
 
@@ -290,55 +290,86 @@
         s = {0: SELF, 1: RIGHT, 3: LEFT, 2: OPP}[step]
         return GX.at[pl.ds(s * block, block), pl.ds(which * (width // 2), width // 2)]
 
-    A1, A2 = 384, 2 * hid - 384
-    B = PB.shape[0]
+    def strip(buf, count):
+        def piece(step):
+            row = pl.multiple_of(turn(rep, step) * (count // 4), 16)
+            return buf.at[pl.ds(row, count // 4)]
+        return piece
+
+    def column(buf):
+        def piece(step):
+            return buf.at[:, lanes_of(step)]
+        return piece
+
+    class Exchange:
+        def __init__(self, piece, bufs, dest):
+            self.piece, self.bufs, self.dest = piece, bufs, dest
+
+        def start(self):
+            self.keys = [
+                (send(self.piece(step), self.bufs[step - 1], self.dest(step)), self.bufs[step - 1])
+                for step in (2, 1, 3)
+            ]
+
+        def finish(self, start):
+            for k, landing in self.keys:
+                arrived(k, landing)
+            total = self.piece(0)[...].astype(F32)
+            for buf in self.bufs:
+                total = total + buf[...].astype(F32)
+            OUTT[pl.ds(start, total.shape[0]), :] = total.astype(BF16)
+
+    class Gather:
+        def __init__(self, base, count):
+            self.base, self.count = base, count // 4
+
+        def row(self, step):
+            return pl.multiple_of(self.base + turn(rep, step) * self.count, 16)
+
+        def region(self, step):
+            return OUTT.at[pl.ds(self.row(step), self.count)]
+
+        def start(self):
+            self.keys = [
+                (send(self.region(0), self.region(0), at_z(step)), 4 - step) for step in (2, 1, 3)
+            ]
+
+        def finish(self):
+            for k, step in self.keys:
+                arrived(k, self.region(step))
+
+    (A1, A2), (B1, B2) = SPLIT
+    b1, b2 = A1 + A2, A1 + A2 + B1
     ya1 = Ring(y_piece(PW, 0, A1), ring_bufs[0:4], at_y)
     ya2 = Ring(y_piece(PW, A1, A2), ring_bufs[4:8], at_y)
-    zb = Ring(z_piece(PB, B // 4, width // 2), ring_bufs[8:12], at_z)
-    za1 = Ring(z_piece(YA1, A1 // 4, shard // 2), ring_bufs[12:16], at_z)
-    za2 = Ring(z_piece(YA2, A2 // 4, shard // 2), ring_bufs[16:20], at_z)
-    yb = Ring(y_piece(ZB, 0, B // 4), ring_bufs[20:24], at_y)
-    xr = Ring(x_piece, ring_bufs[24:28], at_x)
-
-    def to_rows(buf, start):
+    zb1 = Ring(z_piece(PW, b1, B1 // 4, width // 2), ring_bufs[8:12], at_z)
+    zb2 = Ring(z_piece(PW, b2, B2 // 4, width // 2), ring_bufs[12:16], at_z)
+    xr = Ring(x_piece, ring_bufs[16:20], at_x)
+    za1 = Exchange(strip(YA1, A1), ring_bufs[20:23], at_z)
+    za2 = Exchange(strip(YA2, A2), ring_bufs[23:26], at_z)
+    yb1 = Exchange(column(ZB1), ring_bufs[26:29], at_y)
+    yb2 = Exchange(column(ZB2), ring_bufs[29:32], at_y)
+    ga1, ga2, gb1, gb2 = Gather(0, A1), Gather(A1, A2), Gather(b1, B1), Gather(b2, B2)
+
+    def keep(buf):
         def store(which, value):
-            n, h = value.shape
-            buf[pl.ds(start, n), pl.ds(which * h, h)] = value
+            h = value.shape[1]
+            buf[:, pl.ds(which * h, h)] = value
         return store
-
-    class Gather:
-        def __init__(self, base, count):
-            self.base, self.count = base, count
-
-        def row(self, step):
-            return pl.multiple_of(self.base + turn(rep, step) * self.count, 16)
-
-        def region(self, step, which=None):
-            if which is None:
-                return OUTT.at[pl.ds(self.row(step), self.count)]
-            return OUTT.at[pl.ds(self.row(step), self.count), pl.ds(which * (shard // 2), shard // 2)]
-
-        def start(self):
-            self.a = send(self.region(0), self.region(0), at_z(1))
-            self.b = send(self.region(0), self.region(0), at_z(3))
-
-        def relay(self):
-            arrived(self.a, self.region(3))
-            self.c = send(self.region(3, 0), self.region(3, 0), at_z(1))
-            arrived(self.b, self.region(1))
-            self.d = send(self.region(1, 1), self.region(1, 1), at_z(3))
-
-        def finish(self):
-            arrived(self.c, self.region(2, 0))
-            arrived(self.d, self.region(2, 1))
-
-    ga1, ga2, gb = Gather(0, A1 // 4), Gather(A1, A2 // 4), Gather(2 * hid, B // 4)
 
     def weight_piece(step, start, count):
         lanes = lanes_of(step)
         PW[pl.ds(start, count), lanes] = (
             factor * nn(H[pl.ds(start, count), :], X[:, lanes])
         ).astype(BF16)
+
+    def weight_rows(start, count):
+        for lo, hi, tokens in ((start, min(start + count, 2 * hid), X), (max(start, 2 * hid), min(start + count, 3 * hid), G)):
+            if lo < hi:
+                for n in range(4):
+                    PW[pl.ds(lo, hi - lo), pl.ds(n * 256, 256)] = (
+                        factor * nn(H[pl.ds(lo, hi - lo), :], tokens[:, pl.ds(n * 256, 256)])
+                    ).astype(BF16)
 
     def input_piece(c):
         DX[pl.ds(c * 256, 256), :] = tn(
@@ -356,79 +387,76 @@
             + DS[pl.ds(s * block, block), :].astype(F32)
         ).astype(BF16)
 
+    spare = PW.shape[0] - 3 * hid
+    PW[pl.ds(3 * hid, spare), :] = jnp.zeros((spare, width), BF16)
     weight_piece(2, 0, A1)
     ya1.start_far()
-    PB[pl.ds(hid, B - hid), :] = jnp.zeros((B - hid, width), BF16)
-    for n in range(4):
-        PB[pl.ds(0, hid), pl.ds(n * 256, 256)] = (
-            factor * nn(H[pl.ds(2 * hid, hid), :], G[:, pl.ds(n * 256, 256)])
-        ).astype(BF16)
-    zb.start_far()
-    zb.start_near()
+    weight_rows(b1, B1)
+    zb1.start_far()
+    zb1.start_near()
     weight_piece(1, 0, A1)
     weight_piece(3, 0, A1)
     ya1.start_near()
+    weight_rows(A1, A2)
+    ya2.start_far()
+    weight_rows(b2, B2)
+    zb2.start_far()
     input_piece(2)
     opp = across(OPP)
-    for step in (2, 1, 3, 0):
-        weight_piece(step, A1, A2)
+    input_piece(1)
+    near = across(LEFT), across(RIGHT)
     ya1.relay()
-    ya2.start_far()
     ya2.start_near()
-    zb.relay()
-    weight_piece(0, 0, A1)
+    zb1.relay()
+    zb2.start_near()
     across_add(opp, OPP)
     xr.start_far()
-    input_piece(1)
-    near = across(LEFT), across(RIGHT)
     input_piece(0)
     mine = across(SELF)
     across_add(near[0], LEFT)
     across_add(near[1], RIGHT)
     xr.start_near()
-    ya1.finish(to_rows(YA1, 0))
-    za1.start_far()
-    za1.start_near()
-
-    def zb_store(which, value):
-        ZB[:, pl.ds(which * (width // 2), width // 2)] = value
-
-    zb.finish(zb_store)
+    weight_piece(0, 0, A1)
     ya2.relay()
-    yb.start_far()
-    yb.start_near()
+    zb2.relay()
+    ya1.finish(keep(YA1))
+    za1.start()
+    zb1.finish(keep(ZB1))
+    yb1.start()
+    across_add(mine, SELF)
     xr.relay()
-    across_add(mine, SELF)
-    za1.relay()
-    za1.finish(to_rows(OUTT, ga1.row(0)))
+    ya2.finish(keep(YA2))
+    za2.start()
+    zb2.finish(keep(ZB2))
+    yb2.start()
+    za1.finish(ga1.row(0))
     ga1.start()
-    yb.relay()
-    ya2.finish(to_rows(YA2, 0))
-    za2.start_far()
-    za2.start_near()
-    yb.finish(to_rows(OUTT, gb.row(0)))
-    gb.start()
-    ga1.relay()
-    za2.relay()
-
-    def gin_store(which, value):
-        gin_out[:, pl.ds(which * (width // 2), width // 2)] = value
-
-    xr.finish(gin_store)
-    za2.finish(to_rows(OUTT, ga2.row(0)))
+    yb1.finish(gb1.row(0))
+    gb1.start()
+    za2.finish(ga2.row(0))
     ga2.start()
-    gb.relay()
-    ga1.finish()
-    turned = eye(shard)
-    gb.finish()
+    yb2.finish(gb2.row(0))
+    gb2.start()
+    xr.finish(keep(gin_out))
+    for gather in (ga1, ga2):
+        gather.finish()
+    og_out[...] = OUTT[pl.ds(0, hid), :].astype(F32)
+    for gather in (gb1, gb2):
+        gather.finish()
+    ou_out[...] = OUTT[pl.ds(hid, hid), :].astype(F32)
     od_out[...] = OUTT[pl.ds(2 * hid, hid), :].astype(F32)
-    ga2.relay()
-    og_out[...] = nt(turned, OUTT[pl.ds(0, hid), :])
-    ga2.finish()
-    ou_out[...] = nt(turned, OUTT[pl.ds(hid, hid), :])
 
     for copy in pending:
         copy.wait_send()
+
+
+def writer(*refs):
+    sources, targets, sems = refs[:4], refs[4:8], refs[8]
+    copies = [pltpu.make_async_copy(a, b, sems.at[i]) for i, (a, b) in enumerate(zip(sources, targets))]
+    for copy in copies:
+        copy.start()
+    for copy in copies:
+        copy.wait()
 
 
 def body(tokens_in, out_grad, gate_weight, up_weight, down_weight):
@@ -437,7 +465,8 @@
     devices = lax.axis_size("rep") * lax.axis_size("fs") * lax.axis_size("tp")
     factor = (block * devices) ** (-0.5)
     tokens = block * 8
-    A1, A2, B = 384, 2 * hid - 384, 384
+    (A1, A2), (B1, B2) = SPLIT
+    total_rows = A1 + A2 + B1 + B2
 
     def ring(count, lanes):
         return [
@@ -447,37 +476,41 @@
             pltpu.VMEM((count, lanes), BF16),
         ]
 
+    def exchange(count):
+        return [pltpu.VMEM((count // 4, shard), BF16)] * 3
+
     rings = (
-        ring(A1, shard) + ring(A2, shard) + ring(B // 4, width)
-        + ring(A1 // 4, shard) + ring(A2 // 4, shard) + ring(B // 4, shard)
+        ring(A1, shard) + ring(A2, shard) + ring(B1 // 4, width) + ring(B2 // 4, width)
         + ring(block, width)
+        + exchange(A1) + exchange(A2) + exchange(B1) + exchange(B2)
     )
-    return pl.pallas_call(
+    outs = (
+        jax.ShapeDtypeStruct((block, width), BF16),
+        jax.ShapeDtypeStruct((hid, shard), F32),
+        jax.ShapeDtypeStruct((hid, shard), F32),
+        jax.ShapeDtypeStruct((hid, shard), F32),
+    )
+    results = pl.pallas_call(
         functools.partial(kernel, factor, block, width, hid),
-        out_shape=(
-            jax.ShapeDtypeStruct((block, width), BF16),
-            jax.ShapeDtypeStruct((shard, hid), F32),
-            jax.ShapeDtypeStruct((shard, hid), F32),
-            jax.ShapeDtypeStruct((hid, shard), F32),
-        ),
-        in_specs=[pl.BlockSpec(memory_space=pl.ANY)] * 5,
+        out_shape=outs,
+        in_specs=[pl.BlockSpec(memory_space=pltpu.HBM)] * 5,
         out_specs=[pl.BlockSpec(memory_space=pltpu.VMEM)] * 4,
         scratch_shapes=[
             pltpu.VMEM((tokens, width), BF16),
             pltpu.VMEM((tokens, width), BF16),
             pltpu.VMEM((3 * hid, width), BF16),
-            pltpu.VMEM((shard, hid), BF16),
-            pltpu.VMEM((shard, hid), BF16),
             pltpu.VMEM((3 * hid, tokens), BF16),
-            pltpu.VMEM((2 * hid, width), BF16),
-            pltpu.VMEM((B, width), BF16),
+            pltpu.VMEM((hid, tokens), F32),
+            pltpu.VMEM((hid, tokens), F32),
+            pltpu.VMEM((total_rows, width), BF16),
             pltpu.VMEM((tokens, width), BF16),
             pltpu.VMEM((tokens // 2, width), BF16),
             pltpu.VMEM((tokens // 2, width), BF16),
             pltpu.VMEM((A1, shard), BF16),
             pltpu.VMEM((A2, shard), BF16),
-            pltpu.VMEM((B // 4, width), BF16),
-            pltpu.VMEM((2 * hid + B, shard), BF16),
+            pltpu.VMEM((B1 // 4, width), BF16),
+            pltpu.VMEM((B2 // 4, width), BF16),
+            pltpu.VMEM((total_rows, shard), BF16),
             rings,
             pltpu.SemaphoreType.DMA((COPIES,)),
             pltpu.SemaphoreType.DMA((COPIES,)),
@@ -486,7 +519,16 @@
         compiler_params=pltpu.CompilerParams(
             collective_id=0, has_side_effects=True, vmem_limit_bytes=48 * 1024 * 1024
         ),
-    )(tokens_in, out_grad, gate_weight, up_weight, down_weight)
+    )(tokens_in, out_grad, gate_weight.T, up_weight.T, down_weight)
+    grad_in, gate_t, up_t, down_t = pl.pallas_call(
+        writer,
+        out_shape=outs,
+        in_specs=[pl.BlockSpec(memory_space=pl.ANY)] * 4,
+        out_specs=[pl.BlockSpec(memory_space=pltpu.HBM)] * 4,
+        scratch_shapes=[pltpu.SemaphoreType.DMA((4,))],
+        compiler_params=pltpu.CompilerParams(vmem_limit_bytes=1024 * 1024),
+    )(*results)
+    return grad_in, gate_t.T, up_t.T, down_t
 
 
 def solution(mesh):

time: 70.1 us -> 58.6 us (0.84)
  Pallas kernels: 63.9 us -> 53.1 us
  local copies, waits for them, and re-layouts: 5.33 us -> 4.61 us
    pallas_call x1, Pallas kernels: 63.9 us -> 52.1 us  [body(): pl.pallas_call(functools.partial(kernel, factor, block, width, hid), out_...]
    pallas_call x2 -> x0, local copies, waits for them, and re-layouts: 1.79 us -> none  [body(): pl.pallas_call(functools.partial(kernel, factor, block, width, hid), out_...]
    pallas_call x0 -> x1, Pallas kernels: none -> 1.08 us  [body(): pl.pallas_call(writer, out_shape=outs, in_specs=[pl.BlockSpec(memory_spac...]
    unnamed x12 -> x10, local copies, waits for them, and re-layouts: 3.54 us -> 4.61 us
where the time goes in v2:
time: 58.6 us; the launch traced here: 58.4 us
  Pallas kernels  53.1 us (91%)
  local copies, waits for them, and re-layouts  4.61 us (8%)
  between operations  0.65 us (1%)
    pallas_call x1, Pallas kernels, body(): pl.pallas_call(functools.partial(kernel, factor, block, width, hid), out_...  52.1 us
    unnamed x10, local copies, waits for them, and re-layouts  4.61 us

profile of v2, /device:TPU:0, one launch (start us, length us, event | category | flops | bytes accessed | tf_op | source)
XLA Modules:
  0.0 58.4 jit_solution(16910527344313110861)
XLA Ops:
  0.6 0.0 copy-start
  0.6 0.9 %copy-done = bf16[96,1024]{1,0:T(8,128)(2,1)S(1)} copy-done((bf16[96,1024]{1,0:T(8,128)(2,1)S(1)}, bf16[96,1024]{1,0:T(8,128)(2,1)}, u32[]{:S(2)}) %copy-start) | copy-done | bytes 196632
  1.6 0.0 copy-start.1
  1.6 0.9 %copy-done.1 = bf16[96,1024]{1,0:T(8,128)(2,1)S(1)} copy-done((bf16[96,1024]{1,0:T(8,128)(2,1)S(1)}, bf16[96,1024]{1,0:T(8,128)(2,1)}, u32[]{:S(2)}) %copy-start.1) | copy-done | bytes 196632
  2.5 0.0 copy-start.2
  2.5 0.9 %copy-done.2 = bf16[256,352]{0,1:T(8,128)(2,1)S(1)} copy-done((bf16[256,352]{0,1:T(8,128)(2,1)S(1)}, bf16[256,352]{0,1:T(8,128)(2,1)}, u32[]{:S(2)}) %copy-start.2) | copy-done | bytes 180248
  3.4 0.0 copy-start.3
  3.4 0.9 %copy-done.3 = bf16[256,352]{0,1:T(8,128)(2,1)S(1)} copy-done((bf16[256,352]{0,1:T(8,128)(2,1)S(1)}, bf16[256,352]{0,1:T(8,128)(2,1)}, u32[]{:S(2)}) %copy-start.3) | copy-done | bytes 180248
  4.3 0.0 copy-start.4
  4.3 0.9 %copy-done.4 = bf16[352,256]{1,0:T(8,128)(2,1)S(1)} copy-done((bf16[352,256]{1,0:T(8,128)(2,1)S(1)}, bf16[352,256]{1,0:T(8,128)(2,1)}, u32[]{:S(2)}) %copy-start.4) | copy-done | bytes 180248
  5.3 52.1 %shard_map.84 = (bf16[96,1024]{1,0:T(8,128)(2,1)S(1)}, f32[352,256]{1,0:T(8,128)S(1)}, f32[352,256]{1,0:T(8,128)S(1)}, f32[352,256]{1,0:T(8,128)S(1)}) custom-call(bf16[96,1024]{1,0:T(8,128)(2,1)S(1)} %copy-done, bf16[96,1024]{1,0:T(8,128)(2,1)S(1)} %copy-done.1, bf16[352,256]{1,0:T(8,128)(2,1)S(1)} %bitcast.4, bf16[352,256]{1,0:T(8,128)(2,1)S(1)} %bitcast.5, ...), custom_call_target="tpu_custom_call" | custom-call | tf_op jit(solution)/shard_map/pallas_call | solution.py:493
  57.3 1.1 %shard_map.85 = (bf16[96,1024]{1,0:T(8,128)(2,1)}, f32[352,256]{1,0:T(8,128)}, f32[352,256]{1,0:T(8,128)}, f32[352,256]{1,0:T(8,128)}) custom-call(bf16[96,1024]{1,0:T(8,128)(2,1)S(1)} %get-tuple-element.12.refs_0_, f32[352,256]{1,0:T(8,128)S(1)} %get-tuple-element.13.refs_1_, f32[352,256]{1,0:T(8,128)S(1)} %get-tuple-element.14.refs_2_, ...), custom_call_target="tpu_custom_call" | custom-call | tf_op jit(solution)/shard_map/pallas_call | solution.py:523
Async XLA Ops:
  0.6 0.9 %copy-start = (bf16[96,1024]{1,0:T(8,128)(2,1)S(1)}, bf16[96,1024]{1,0:T(8,128)(2,1)}, u32[]{:S(2)}) copy-start(bf16[96,1024]{1,0:T(8,128)(2,1)} %x_in.1) | copy-start | bytes 589828
  1.6 0.9 %copy-start.1 = (bf16[96,1024]{1,0:T(8,128)(2,1)S(1)}, bf16[96,1024]{1,0:T(8,128)(2,1)}, u32[]{:S(2)}) copy-start(bf16[96,1024]{1,0:T(8,128)(2,1)} %g_in.1) | copy-start | bytes 589828
  2.5 0.9 %copy-start.2 = (bf16[256,352]{0,1:T(8,128)(2,1)S(1)}, bf16[256,352]{0,1:T(8,128)(2,1)}, u32[]{:S(2)}) copy-start(bf16[256,352]{0,1:T(8,128)(2,1)} %param.7) | copy-start | bytes 540676
  3.4 0.9 %copy-start.3 = (bf16[256,352]{0,1:T(8,128)(2,1)S(1)}, bf16[256,352]{0,1:T(8,128)(2,1)}, u32[]{:S(2)}) copy-start(bf16[256,352]{0,1:T(8,128)(2,1)} %param.8) | copy-start | bytes 540676
  4.3 0.9 %copy-start.4 = (bf16[352,256]{1,0:T(8,128)(2,1)S(1)}, bf16[352,256]{1,0:T(8,128)(2,1)}, u32[]{:S(2)}) copy-start(bf16[352,256]{1,0:T(8,128)(2,1)} %wd_in.1) | copy-start | bytes 540676

commit v3 on v2

--- a/solution.py
+++ b/solution.py
@@ -78,6 +78,12 @@
     def arrived(k, landing):
         remote(landing, landing, k, sibling).wait_recv()
 
+    barrier = pltpu.get_barrier_semaphore()
+    partners = [sibling] + [at(step) for at in (at_x, at_y, at_z) for step in (1, 3)]
+    partners += [at_y(2), at_z(2)]
+    for where in partners:
+        pl.semaphore_signal(barrier, inc=1, device_id=where, device_id_type=MESH)
+
     own_lanes = lanes_of(0)
     loads = [
         pltpu.make_async_copy(x_in, X.at[pl.ds(0, block)], local_sems.at[0]),
@@ -89,10 +95,7 @@
     for load in loads:
         load.start()
 
-    barrier = pltpu.get_barrier_semaphore()
-    for where in (at_x(1), at_x(3), at_y(1), at_y(3), at_z(1), at_z(3), sibling):
-        pl.semaphore_signal(barrier, inc=1, device_id=where, device_id_type=MESH)
-    pl.semaphore_wait(barrier, 7)
+    pl.semaphore_wait(barrier, len(partners))
 
     half = block // 2
     SELF, LEFT, RIGHT, OPP = 0, 1, 2, 3
@@ -100,110 +103,135 @@
     def slot(buf, s, start=0, count=block):
         return buf.at[pl.ds(s * 2 * block + start, count)]
 
-    def token_start(buf):
-        right = send(slot(buf, SELF), slot(buf, LEFT), at_x(1))
-        left = send(slot(buf, SELF), slot(buf, RIGHT), at_x(3))
-        across = send(slot(buf, SELF), slot(buf, SELF, block), sibling)
-        return right, left, [(across, (SELF, block))]
-
-    def token_relay(buf, state):
-        right, left, across = state
-        arrived(right, slot(buf, LEFT))
-        right = send(slot(buf, LEFT, 0, half), slot(buf, OPP, 0, half), at_x(1))
-        arrived(left, slot(buf, RIGHT))
-        left = send(slot(buf, RIGHT, half, half), slot(buf, OPP, half, half), at_x(3))
-        across.append((send(slot(buf, LEFT), slot(buf, LEFT, block), sibling), (LEFT, block)))
-        across.append((send(slot(buf, RIGHT), slot(buf, RIGHT, block), sibling), (RIGHT, block)))
-        return right, left, across
-
-    def token_last(buf, state):
-        out = []
-        for k, start in ((state[0], 0), (state[1], half)):
-            arrived(k, slot(buf, OPP, start, half))
-            landing = (OPP, block + start, half)
-            out.append((send(slot(buf, OPP, start, half), slot(buf, *landing), sibling), landing))
-        return out
-
-    def token_wait(buf, across):
-        for k, landing in across:
+    def forward(buf, s, start=0, count=block):
+        landing = (s, block + start, count)
+        return send(slot(buf, s, start, count), slot(buf, *landing), sibling), landing
+
+    def forwarded(buf, *states):
+        for k, landing in states:
             arrived(k, slot(buf, *landing))
 
+    class Tokens:
+        def __init__(self, buf):
+            self.buf = buf
+
+        def part(self, s, which):
+            return slot(self.buf, s, which * half, half)
+
+        def start_first(self):
+            self.r0 = send(self.part(SELF, 0), self.part(LEFT, 0), at_x(1))
+            self.l1 = send(self.part(SELF, 1), self.part(RIGHT, 1), at_x(3))
+
+        def start_second(self):
+            self.r1 = send(self.part(SELF, 1), self.part(LEFT, 1), at_x(1))
+            self.l0 = send(self.part(SELF, 0), self.part(RIGHT, 0), at_x(3))
+
+        def relay(self):
+            arrived(self.r0, self.part(LEFT, 0))
+            self.r2 = send(self.part(LEFT, 0), self.part(OPP, 0), at_x(1))
+            arrived(self.l1, self.part(RIGHT, 1))
+            self.l2 = send(self.part(RIGHT, 1), self.part(OPP, 1), at_x(3))
+
+        def near(self):
+            arrived(self.r1, self.part(LEFT, 1))
+            arrived(self.l0, self.part(RIGHT, 0))
+            return forward(self.buf, LEFT), forward(self.buf, RIGHT)
+
+        def far(self):
+            arrived(self.r2, self.part(OPP, 0))
+            first = forward(self.buf, OPP, 0, half)
+            arrived(self.l2, self.part(OPP, 1))
+            return first, forward(self.buf, OPP, half, half)
+
+    xt, gt = Tokens(X), Tokens(G)
     loads[0].wait()
-    x_state = token_start(X)
+    xt.start_first()
+    xt.start_second()
     loads[1].wait()
-    g_state = token_start(G)
-
+    gt.start_first()
     for load in loads[2:]:
         load.wait()
 
-    direct = 544
-    part = (3 * hid - direct) // 4
-    dhalf = direct // 2
+    part, direct, spare = 64, 448, 96
+    base1, base2 = direct, 2 * hid + spare
+    qh, dhalf = part // 2, direct // 2
     D0, D1 = pl.ds(0, dhalf), pl.ds(dhalf, dhalf)
-
-    def quarter(step, start=0, count=part):
-        return pl.ds(pl.multiple_of(direct + turn(rep, step) * part + start, 16), count)
+    D2 = pl.ds(2 * hid, spare)
+
+    def quarter(base, step, start=0, count=part):
+        return pl.ds(pl.multiple_of(base + turn(rep, step) * part + start, 16), count)
 
     def w(rows, step):
         return WT.at[rows, lanes_of(step)]
 
-    qa = send(w(quarter(0), 0), w(quarter(0), 0), at_y(1))
-    qb = send(w(quarter(0), 0), w(quarter(0), 0), at_y(3))
-    d0r = send(w(D0, 0), w(D0, 0), at_y(1))
-    d1l = send(w(D1, 0), w(D1, 0), at_y(3))
-
-    qh = part // 2
-    arrived(qa, w(quarter(0), 3))
-    qc = send(w(quarter(0, 0, qh), 3), w(quarter(0, 0, qh), 3), at_y(1))
-    arrived(qb, w(quarter(0), 1))
-    qd = send(w(quarter(0, qh, qh), 1), w(quarter(0, qh, qh), 1), at_y(3))
-    d1r = send(w(D1, 0), w(D1, 0), at_y(1))
-    d0l = send(w(D0, 0), w(D0, 0), at_y(3))
-
-    def share(step):
-        return (
-            send(w(quarter(0), step), w(quarter(0), step), at_z(1)),
-            send(w(quarter(0), step), w(quarter(0), step), at_z(3)),
-        )
-
-    def share_relay(state, step):
-        arrived(state[0], w(quarter(3), step))
-        a = send(w(quarter(3, 0, qh), step), w(quarter(3, 0, qh), step), at_z(1))
-        arrived(state[1], w(quarter(1), step))
-        b = send(w(quarter(1, qh, qh), step), w(quarter(1, qh, qh), step), at_z(3))
-        return a, b
-
-    def share_last(state, step):
-        arrived(state[0], w(quarter(2, 0, qh), step))
-        arrived(state[1], w(quarter(2, qh, qh), step))
-
-    z3 = share(3)
-    z1 = share(1)
-
-    x_state = token_relay(X, x_state)
-
+    def copy_w(rows, step, where):
+        return send(w(rows, step), w(rows, step), where)
+
+    class Quarters:
+        def __init__(self, base):
+            self.base = base
+
+        def start(self):
+            own = quarter(self.base, 0)
+            self.r, self.l = copy_w(own, 0, at_y(1)), copy_w(own, 0, at_y(3))
+            self.shares = {}
+
+        def relay(self):
+            arrived(self.r, w(quarter(self.base, 0), 3))
+            self.r2 = copy_w(quarter(self.base, 0, 0, qh), 3, at_y(1))
+            arrived(self.l, w(quarter(self.base, 0), 1))
+            self.l2 = copy_w(quarter(self.base, 0, qh, qh), 1, at_y(3))
+
+        def far(self):
+            arrived(self.r2, w(quarter(self.base, 0, 0, qh), 2))
+            arrived(self.l2, w(quarter(self.base, 0, qh, qh), 2))
+
+        def share(self, lane):
+            self.shares[lane] = [
+                (copy_w(quarter(self.base, 0), lane, at_z(step)), 4 - step) for step in (2, 1, 3)
+            ]
+
+        def finish(self):
+            for lane, keys in self.shares.items():
+                for k, step in keys:
+                    arrived(k, w(quarter(self.base, step), lane))
+
+    q1, q2 = Quarters(base1), Quarters(base2)
+    q1.start()
+    q2.start()
+    d0r = copy_w(D0, 0, at_y(1))
+    d1l = copy_w(D1, 0, at_y(3))
+    x_own = forward(X, SELF)
+    g_own = forward(G, SELF)
+
+    q1.relay()
+    q1.share(3)
+    q1.share(1)
+    q2.relay()
+    d1r = copy_w(D1, 0, at_y(1))
+    d0l = copy_w(D0, 0, at_y(3))
+
+    xt.relay()
+    gt.start_second()
     arrived(d0r, w(D0, 3))
-    dc = send(w(D0, 3), w(D0, 3), at_y(1))
+    dc = copy_w(D0, 3, at_y(1))
     arrived(d1l, w(D1, 1))
-    dd = send(w(D1, 1), w(D1, 1), at_y(3))
-
-    z3 = share_relay(z3, 3)
-    arrived(qc, w(quarter(0, 0, qh), 2))
-    arrived(qd, w(quarter(0, qh, qh), 2))
-    z2 = share(2)
-    z1 = share_relay(z1, 1)
-
-    g_state = token_relay(G, g_state)
-    x_last = token_last(X, x_state)
-    z2 = share_relay(z2, 2)
-
-    token_wait(X, x_state[2])
-    token_wait(X, x_last)
-    token_wait(G, g_state[2])
+    dd = copy_w(D1, 1, at_y(3))
+    x_near = xt.near()
+    q1.far()
+    q1.share(2)
+    q2.share(3)
+    q2.share(1)
+    q2.far()
+    q2.share(2)
+    d2 = [(copy_w(D2, 0, at_y(step)), 4 - step) for step in (2, 1, 3)]
+    gt.relay()
+    x_far = xt.far()
+
+    forwarded(X, x_own, *x_near)
     arrived(d1r, w(D1, 3))
     arrived(d0l, w(D0, 1))
-    for state, step in ((z3, 3), (z1, 1), (z2, 2)):
-        share_last(state, step)
+    q1.finish()
     arrived(dc, w(D0, 2))
     arrived(dd, w(D1, 2))
 
@@ -229,11 +257,18 @@
 
     gate_stage(0)
     gate_stage(1)
-    g_last = token_last(G, g_state)
+    g_near = gt.near()
+    forwarded(X, *x_far)
     gate_stage(2)
+    q2.finish()
+    for k, step in d2:
+        arrived(k, w(D2, step))
+    forwarded(G, g_own, g_near[0])
     grad_stage(0)
+    g_far = gt.far()
+    forwarded(G, g_near[1])
     grad_stage(1)
-    token_wait(G, g_last)
+    forwarded(G, *g_far)
     grad_stage(2)
 
     class Ring:
@@ -387,8 +422,8 @@
             + DS[pl.ds(s * block, block), :].astype(F32)
         ).astype(BF16)
 
-    spare = PW.shape[0] - 3 * hid
-    PW[pl.ds(3 * hid, spare), :] = jnp.zeros((spare, width), BF16)
+    blank = PW.shape[0] - 3 * hid
+    PW[pl.ds(3 * hid, blank), :] = jnp.zeros((blank, width), BF16)
     weight_piece(2, 0, A1)
     ya1.start_far()
     weight_rows(b1, B1)
@@ -490,6 +525,7 @@
         jax.ShapeDtypeStruct((hid, shard), F32),
         jax.ShapeDtypeStruct((hid, shard), F32),
     )
+    arrays = tokens_in, out_grad, gate_weight.T, up_weight.T, down_weight
     results = pl.pallas_call(
         functools.partial(kernel, factor, block, width, hid),
         out_shape=outs,
@@ -519,7 +555,7 @@
         compiler_params=pltpu.CompilerParams(
             collective_id=0, has_side_effects=True, vmem_limit_bytes=48 * 1024 * 1024
         ),
-    )(tokens_in, out_grad, gate_weight.T, up_weight.T, down_weight)
+    )(*[pltpu.with_memory_space_constraint(a, pltpu.HBM) for a in arrays])
     grad_in, gate_t, up_t, down_t = pl.pallas_call(
         writer,
         out_shape=outs,

time: 58.6 us -> 50.7 us (0.87)
  local copies, waits for them, and re-layouts: 4.61 us -> 0 us
  Pallas kernels: 53.1 us -> 49.9 us
    unnamed x10 -> x0, local copies, waits for them, and re-layouts: 4.61 us -> none
    pallas_call x1, Pallas kernels: 52.1 us -> 48.9 us  [body(): pl.pallas_call(functools.partial(kernel, factor, block, width, hid), out_...]
where the time goes in v3:
time: 50.7 us; the launch traced here: 50.6 us
  Pallas kernels  49.9 us (98%)
  between operations  0.64 us (1%)
    pallas_call x1, Pallas kernels, body(): pl.pallas_call(functools.partial(kernel, factor, block, width, hid), out_...  48.9 us
    pallas_call x1, Pallas kernels, body(): pl.pallas_call(writer, out_shape=outs, in_specs=[pl.BlockSpec(memory_spac...  1.08 us

profile of v3, /device:TPU:0, one launch (start us, length us, event | category | flops | bytes accessed | tf_op | source)
XLA Modules:
  0.0 50.6 jit_solution(3596749830571953546)
XLA Ops:
  0.6 48.9 %shard_map.84 = (bf16[96,1024]{1,0:T(8,128)(2,1)S(1)}, f32[352,256]{1,0:T(8,128)S(1)}, f32[352,256]{1,0:T(8,128)S(1)}, f32[352,256]{1,0:T(8,128)S(1)}) custom-call(bf16[96,1024]{1,0:T(8,128)(2,1)} %x_in.1, bf16[96,1024]{1,0:T(8,128)(2,1)} %g_in.1, bf16[352,256]{1,0:T(8,128)(2,1)} %bitcast.4, bf16[352,256]{1,0:T(8,128)(2,1)} %bitcast.5, bf16[352,256]{1,0:T(8,128)(2,1)} %wd_in.1), custom_call_target="tpu_custom_call" | custom-call | tf_op jit(solution)/shard_map/pallas_call | solution.py:529
  49.5 1.1 %shard_map.85 = (bf16[96,1024]{1,0:T(8,128)(2,1)}, f32[352,256]{1,0:T(8,128)}, f32[352,256]{1,0:T(8,128)}, f32[352,256]{1,0:T(8,128)}) custom-call(bf16[96,1024]{1,0:T(8,128)(2,1)S(1)} %get-tuple-element.12.refs_0_, f32[352,256]{1,0:T(8,128)S(1)} %get-tuple-element.13.refs_1_, f32[352,256]{1,0:T(8,128)S(1)} %get-tuple-element.14.refs_2_, ...), custom_call_target="tpu_custom_call" | custom-call | tf_op jit(solution)/shard_map/pallas_call | solution.py:559

commit v4 on v3

--- a/solution.py
+++ b/solution.py
@@ -10,8 +10,8 @@
 BF16 = jnp.bfloat16
 F32 = jnp.float32
 MESH = pl.DeviceIdType.MESH
-COPIES = 128
-SPLIT = (320, 256), (256, 256)
+COPIES = 144
+SPLIT = (128, 256, 192), (128, 192, 192)
 
 
 def nt(left, right):
@@ -30,8 +30,7 @@
     factor, block, width, hid,
     x_in, g_in, wg_in, wu_in, wd_in,
     gin_out, og_out, ou_out, od_out,
-    X, G, WT, H, ACT, SLOPE, PW, DX, DS, GX, YA1, YA2, ZB1, ZB2, OUTT,
-    ring_bufs,
+    X, G, WT, H, ACT, SLOPE, PW, DX, DS, GX, YA, ZB, OUTT, YA_BUFS, ZB_BUFS, ZA_BUFS, YB_BUFS, XR_BUFS,
     send_sems, recv_sems, local_sems,
 ):
     rep = lax.axis_index("rep")
@@ -152,15 +151,12 @@
     for load in loads[2:]:
         load.wait()
 
-    part, direct, spare = 64, 448, 96
+    direct, spare = 384, 96
     base1, base2 = direct, 2 * hid + spare
-    qh, dhalf = part // 2, direct // 2
+    dhalf = direct // 2
     D0, D1 = pl.ds(0, dhalf), pl.ds(dhalf, dhalf)
     D2 = pl.ds(2 * hid, spare)
 
-    def quarter(base, step, start=0, count=part):
-        return pl.ds(pl.multiple_of(base + turn(rep, step) * part + start, 16), count)
-
     def w(rows, step):
         return WT.at[rows, lanes_of(step)]
 
@@ -168,35 +164,41 @@
         return send(w(rows, step), w(rows, step), where)
 
     class Quarters:
-        def __init__(self, base):
-            self.base = base
+        def __init__(self, base, end):
+            self.base, self.part = base, (end - base) // 4
+            self.cut = (self.part // 2 + 15) // 16 * 16
+
+        def rows(self, step, which=None):
+            start, count = {
+                None: (0, self.part), 0: (0, self.cut), 1: (self.cut, self.part - self.cut)
+            }[which]
+            return pl.ds(pl.multiple_of(self.base + turn(rep, step) * self.part + start, 16), count)
 
         def start(self):
-            own = quarter(self.base, 0)
-            self.r, self.l = copy_w(own, 0, at_y(1)), copy_w(own, 0, at_y(3))
+            self.r, self.l = copy_w(self.rows(0), 0, at_y(1)), copy_w(self.rows(0), 0, at_y(3))
             self.shares = {}
 
         def relay(self):
-            arrived(self.r, w(quarter(self.base, 0), 3))
-            self.r2 = copy_w(quarter(self.base, 0, 0, qh), 3, at_y(1))
-            arrived(self.l, w(quarter(self.base, 0), 1))
-            self.l2 = copy_w(quarter(self.base, 0, qh, qh), 1, at_y(3))
+            arrived(self.r, w(self.rows(0), 3))
+            self.r2 = copy_w(self.rows(0, 0), 3, at_y(1))
+            arrived(self.l, w(self.rows(0), 1))
+            self.l2 = copy_w(self.rows(0, 1), 1, at_y(3))
 
         def far(self):
-            arrived(self.r2, w(quarter(self.base, 0, 0, qh), 2))
-            arrived(self.l2, w(quarter(self.base, 0, qh, qh), 2))
+            arrived(self.r2, w(self.rows(0, 0), 2))
+            arrived(self.l2, w(self.rows(0, 1), 2))
 
         def share(self, lane):
             self.shares[lane] = [
-                (copy_w(quarter(self.base, 0), lane, at_z(step)), 4 - step) for step in (2, 1, 3)
+                (copy_w(self.rows(0), lane, at_z(step)), 4 - step) for step in (2, 1, 3)
             ]
 
         def finish(self):
             for lane, keys in self.shares.items():
                 for k, step in keys:
-                    arrived(k, w(quarter(self.base, step), lane))
-
-    q1, q2 = Quarters(base1), Quarters(base2)
+                    arrived(k, w(self.rows(step), lane))
+
+    q1, q2 = Quarters(base1, 2 * hid), Quarters(base2, 3 * hid)
     q1.start()
     q2.start()
     d0r = copy_w(D0, 0, at_y(1))
@@ -264,8 +266,8 @@
     for k, step in d2:
         arrived(k, w(D2, step))
     forwarded(G, g_own, g_near[0])
+    g_far = gt.far()
     grad_stage(0)
-    g_far = gt.far()
     forwarded(G, g_near[1])
     grad_stage(1)
     forwarded(G, *g_far)
@@ -373,18 +375,16 @@
             for k, step in self.keys:
                 arrived(k, self.region(step))
 
-    (A1, A2), (B1, B2) = SPLIT
-    b1, b2 = A1 + A2, A1 + A2 + B1
-    ya1 = Ring(y_piece(PW, 0, A1), ring_bufs[0:4], at_y)
-    ya2 = Ring(y_piece(PW, A1, A2), ring_bufs[4:8], at_y)
-    zb1 = Ring(z_piece(PW, b1, B1 // 4, width // 2), ring_bufs[8:12], at_z)
-    zb2 = Ring(z_piece(PW, b2, B2 // 4, width // 2), ring_bufs[12:16], at_z)
-    xr = Ring(x_piece, ring_bufs[16:20], at_x)
-    za1 = Exchange(strip(YA1, A1), ring_bufs[20:23], at_z)
-    za2 = Exchange(strip(YA2, A2), ring_bufs[23:26], at_z)
-    yb1 = Exchange(column(ZB1), ring_bufs[26:29], at_y)
-    yb2 = Exchange(column(ZB2), ring_bufs[29:32], at_y)
-    ga1, ga2, gb1, gb2 = Gather(0, A1), Gather(A1, A2), Gather(b1, B1), Gather(b2, B2)
+    A, B = SPLIT
+    a_at = [sum(A[:i]) for i in range(len(A))]
+    b_at = [sum(A) + sum(B[:i]) for i in range(len(B))]
+    ya = [Ring(y_piece(PW, r, n), bufs, at_y) for r, n, bufs in zip(a_at, A, YA_BUFS)]
+    zb = [Ring(z_piece(PW, r, n // 4, width // 2), bufs, at_z) for r, n, bufs in zip(b_at, B, ZB_BUFS)]
+    za = [Exchange(strip(buf, n), bufs, at_z) for buf, n, bufs in zip(YA, A, ZA_BUFS)]
+    yb = [Exchange(column(buf), bufs, at_y) for buf, bufs in zip(ZB, YB_BUFS)]
+    ga = [Gather(r, n) for r, n in zip(a_at, A)]
+    gb = [Gather(r, n) for r, n in zip(b_at, B)]
+    xr = Ring(x_piece, XR_BUFS, at_x)
 
     def keep(buf):
         def store(which, value):
@@ -424,60 +424,78 @@
 
     blank = PW.shape[0] - 3 * hid
     PW[pl.ds(3 * hid, blank), :] = jnp.zeros((blank, width), BF16)
-    weight_piece(2, 0, A1)
-    ya1.start_far()
-    weight_rows(b1, B1)
-    zb1.start_far()
-    zb1.start_near()
-    weight_piece(1, 0, A1)
-    weight_piece(3, 0, A1)
-    ya1.start_near()
-    weight_rows(A1, A2)
-    ya2.start_far()
-    weight_rows(b2, B2)
-    zb2.start_far()
+    weight_piece(2, 0, A[0])
+    ya[0].start_far()
+    weight_rows(b_at[0], B[0])
+    zb[0].start_far()
+    weight_piece(1, 0, A[0])
+    weight_piece(3, 0, A[0])
+    ya[0].start_near()
+    weight_rows(a_at[1], A[1])
+    zb[0].start_near()
+    weight_rows(b_at[1], B[1])
+    ya[1].start_far()
+    weight_rows(a_at[2], A[2])
+    zb[1].start_far()
+    weight_rows(b_at[2], B[2])
     input_piece(2)
     opp = across(OPP)
+    ya[1].start_near()
+    zb[1].start_near()
     input_piece(1)
     near = across(LEFT), across(RIGHT)
-    ya1.relay()
-    ya2.start_near()
-    zb1.relay()
-    zb2.start_near()
+    ya[0].relay()
+    input_piece(0)
+    mine = across(SELF)
+    zb[0].relay()
+    weight_piece(0, 0, A[0])
     across_add(opp, OPP)
     xr.start_far()
-    input_piece(0)
-    mine = across(SELF)
+    zb[2].start_far()
+    ya[2].start_far()
     across_add(near[0], LEFT)
     across_add(near[1], RIGHT)
     xr.start_near()
-    weight_piece(0, 0, A1)
-    ya2.relay()
-    zb2.relay()
-    ya1.finish(keep(YA1))
-    za1.start()
-    zb1.finish(keep(ZB1))
-    yb1.start()
+    ya[1].relay()
+    zb[1].relay()
     across_add(mine, SELF)
+    zb[2].start_near()
+    zb[0].finish(keep(ZB[0]))
+    yb[0].start()
+    ya[0].finish(keep(YA[0]))
+    za[0].start()
+    ya[2].start_near()
+    zb[2].relay()
+    ya[2].relay()
     xr.relay()
-    ya2.finish(keep(YA2))
-    za2.start()
-    zb2.finish(keep(ZB2))
-    yb2.start()
-    za1.finish(ga1.row(0))
-    ga1.start()
-    yb1.finish(gb1.row(0))
-    gb1.start()
-    za2.finish(ga2.row(0))
-    ga2.start()
-    yb2.finish(gb2.row(0))
-    gb2.start()
+    zb[1].finish(keep(ZB[1]))
+    yb[1].start()
+    ya[1].finish(keep(YA[1]))
+    za[1].start()
+    yb[0].finish(gb[0].row(0))
+    gb[0].start()
+    za[0].finish(ga[0].row(0))
+    ga[0].start()
+    zb[2].finish(keep(ZB[2]))
+    yb[2].start()
+    ya[2].finish(keep(YA[2]))
+    za[2].start()
     xr.finish(keep(gin_out))
-    for gather in (ga1, ga2):
-        gather.finish()
+    yb[1].finish(gb[1].row(0))
+    gb[1].start()
+    za[1].finish(ga[1].row(0))
+    ga[1].start()
+    gb[0].finish()
+    ga[0].finish()
+    yb[2].finish(gb[2].row(0))
+    gb[2].start()
+    za[2].finish(ga[2].row(0))
+    ga[2].start()
+    gb[1].finish()
+    ga[1].finish()
+    gb[2].finish()
+    ga[2].finish()
     og_out[...] = OUTT[pl.ds(0, hid), :].astype(F32)
-    for gather in (gb1, gb2):
-        gather.finish()
     ou_out[...] = OUTT[pl.ds(hid, hid), :].astype(F32)
     od_out[...] = OUTT[pl.ds(2 * hid, hid), :].astype(F32)
 
@@ -500,8 +518,8 @@
     devices = lax.axis_size("rep") * lax.axis_size("fs") * lax.axis_size("tp")
     factor = (block * devices) ** (-0.5)
     tokens = block * 8
-    (A1, A2), (B1, B2) = SPLIT
-    total_rows = A1 + A2 + B1 + B2
+    A, B = SPLIT
+    total_rows = sum(A) + sum(B)
 
     def ring(count, lanes):
         return [
@@ -514,11 +532,6 @@
     def exchange(count):
         return [pltpu.VMEM((count // 4, shard), BF16)] * 3
 
-    rings = (
-        ring(A1, shard) + ring(A2, shard) + ring(B1 // 4, width) + ring(B2 // 4, width)
-        + ring(block, width)
-        + exchange(A1) + exchange(A2) + exchange(B1) + exchange(B2)
-    )
     outs = (
         jax.ShapeDtypeStruct((block, width), BF16),
         jax.ShapeDtypeStruct((hid, shard), F32),
@@ -542,12 +555,14 @@
             pltpu.VMEM((tokens, width), BF16),
             pltpu.VMEM((tokens // 2, width), BF16),
             pltpu.VMEM((tokens // 2, width), BF16),
-            pltpu.VMEM((A1, shard), BF16),
-            pltpu.VMEM((A2, shard), BF16),
-            pltpu.VMEM((B1 // 4, width), BF16),
-            pltpu.VMEM((B2 // 4, width), BF16),
+            [pltpu.VMEM((n, shard), BF16) for n in A],
+            [pltpu.VMEM((n // 4, width), BF16) for n in B],
             pltpu.VMEM((total_rows, shard), BF16),
-            rings,
+            [ring(n, shard) for n in A],
+            [ring(n // 4, width) for n in B],
+            [exchange(n) for n in A],
+            [exchange(n) for n in B],
+            ring(block, width),
             pltpu.SemaphoreType.DMA((COPIES,)),
             pltpu.SemaphoreType.DMA((COPIES,)),
             pltpu.SemaphoreType.DMA((5,)),

time: 50.7 us -> 50.1 us (0.988)
  Pallas kernels: 49.9 us -> 49.3 us
    pallas_call x1, Pallas kernels: 48.9 us -> 48.2 us  [body(): pl.pallas_call(functools.partial(kernel, factor, block, width, hid), out_...]
where the time goes in v4:
time: 50.1 us; the launch traced here: 50 us
  Pallas kernels  49.3 us (98%)
  between operations  0.64 us (1%)
    pallas_call x1, Pallas kernels, body(): pl.pallas_call(functools.partial(kernel, factor, block, width, hid), out_...  48.2 us
    pallas_call x1, Pallas kernels, body(): pl.pallas_call(writer, out_shape=outs, in_specs=[pl.BlockSpec(memory_spac...  1.08 us

profile of v4, /device:TPU:0, one launch (start us, length us, event | category | flops | bytes accessed | tf_op | source)
XLA Modules:
  0.0 50.0 jit_solution(4897704843430569567)
XLA Ops:
  0.6 48.2 %shard_map.84 = (bf16[96,1024]{1,0:T(8,128)(2,1)S(1)}, f32[352,256]{1,0:T(8,128)S(1)}, f32[352,256]{1,0:T(8,128)S(1)}, f32[352,256]{1,0:T(8,128)S(1)}) custom-call(bf16[96,1024]{1,0:T(8,128)(2,1)} %x_in.1, bf16[96,1024]{1,0:T(8,128)(2,1)} %g_in.1, bf16[352,256]{1,0:T(8,128)(2,1)} %bitcast.4, bf16[352,256]{1,0:T(8,128)(2,1)} %bitcast.5, bf16[352,256]{1,0:T(8,128)(2,1)} %wd_in.1), custom_call_target="tpu_custom_call" | custom-call | tf_op jit(solution)/shard_map/pallas_call | solution.py:542
  48.9 1.1 %shard_map.85 = (bf16[96,1024]{1,0:T(8,128)(2,1)}, f32[352,256]{1,0:T(8,128)}, f32[352,256]{1,0:T(8,128)}, f32[352,256]{1,0:T(8,128)}) custom-call(bf16[96,1024]{1,0:T(8,128)(2,1)S(1)} %get-tuple-element.12.refs_0_, f32[352,256]{1,0:T(8,128)S(1)} %get-tuple-element.13.refs_1_, f32[352,256]{1,0:T(8,128)S(1)} %get-tuple-element.14.refs_2_, ...), custom_call_target="tpu_custom_call" | custom-call | tf_op jit(solution)/shard_map/pallas_call | solution.py:574

commit v5 on v4

--- a/solution.py
+++ b/solution.py
@@ -11,7 +11,7 @@
 F32 = jnp.float32
 MESH = pl.DeviceIdType.MESH
 COPIES = 144
-SPLIT = (128, 256, 192), (128, 192, 192)
+SPLIT = (192, 192, 192), (128, 256, 128)
 
 
 def nt(left, right):
@@ -429,70 +429,70 @@
     weight_rows(b_at[0], B[0])
     zb[0].start_far()
     weight_piece(1, 0, A[0])
+    zb[0].start_near()
     weight_piece(3, 0, A[0])
     ya[0].start_near()
     weight_rows(a_at[1], A[1])
-    zb[0].start_near()
     weight_rows(b_at[1], B[1])
     ya[1].start_far()
+    zb[1].start_far()
     weight_rows(a_at[2], A[2])
-    zb[1].start_far()
     weight_rows(b_at[2], B[2])
+    ya[1].start_near()
     input_piece(2)
     opp = across(OPP)
-    ya[1].start_near()
-    zb[1].start_near()
+    ya[0].relay()
+    zb[0].relay()
     input_piece(1)
     near = across(LEFT), across(RIGHT)
-    ya[0].relay()
+    zb[1].start_near()
     input_piece(0)
     mine = across(SELF)
-    zb[0].relay()
+    ya[2].start_far()
     weight_piece(0, 0, A[0])
     across_add(opp, OPP)
     xr.start_far()
     zb[2].start_far()
-    ya[2].start_far()
+    ya[1].relay()
+    zb[1].relay()
     across_add(near[0], LEFT)
     across_add(near[1], RIGHT)
     xr.start_near()
-    ya[1].relay()
-    zb[1].relay()
     across_add(mine, SELF)
-    zb[2].start_near()
     zb[0].finish(keep(ZB[0]))
     yb[0].start()
+    zb[2].start_near()
+    ya[2].start_near()
     ya[0].finish(keep(YA[0]))
     za[0].start()
-    ya[2].start_near()
+    ya[2].relay()
     zb[2].relay()
-    ya[2].relay()
     xr.relay()
+    ya[1].finish(keep(YA[1]))
+    za[1].start()
     zb[1].finish(keep(ZB[1]))
     yb[1].start()
-    ya[1].finish(keep(YA[1]))
-    za[1].start()
     yb[0].finish(gb[0].row(0))
     gb[0].start()
     za[0].finish(ga[0].row(0))
     ga[0].start()
+    ya[2].finish(keep(YA[2]))
+    za[2].start()
     zb[2].finish(keep(ZB[2]))
     yb[2].start()
-    ya[2].finish(keep(YA[2]))
-    za[2].start()
-    xr.finish(keep(gin_out))
+    za[1].finish(ga[1].row(0))
+    ga[1].start()
     yb[1].finish(gb[1].row(0))
     gb[1].start()
-    za[1].finish(ga[1].row(0))
-    ga[1].start()
+    xr.finish(keep(gin_out))
     gb[0].finish()
     ga[0].finish()
     yb[2].finish(gb[2].row(0))
     gb[2].start()
     za[2].finish(ga[2].row(0))
     ga[2].start()
+    ga[1].finish()
     gb[1].finish()
-    ga[1].finish()
     gb[2].finish()
     ga[2].finish()
     og_out[...] = OUTT[pl.ds(0, hid), :].astype(F32)

time: 50.1 us -> 50.4 us (level)
  no operation moved by 1% of the time
where the time goes in v5:
time: 50.4 us; the launch traced here: 50.3 us
  Pallas kernels  49.6 us (98%)
  between operations  0.64 us (1%)
    pallas_call x1, Pallas kernels, body(): pl.pallas_call(functools.partial(kernel, factor, block, width, hid), out_...  48.6 us
    pallas_call x1, Pallas kernels, body(): pl.pallas_call(writer, out_shape=outs, in_specs=[pl.BlockSpec(memory_spac...  1.08 us

profile of v5, /device:TPU:0, one launch (start us, length us, event | category | flops | bytes accessed | tf_op | source)
XLA Modules:
  0.0 50.3 jit_solution(968617104118807459)
XLA Ops:
  0.6 48.6 %shard_map.84 = (bf16[96,1024]{1,0:T(8,128)(2,1)S(1)}, f32[352,256]{1,0:T(8,128)S(1)}, f32[352,256]{1,0:T(8,128)S(1)}, f32[352,256]{1,0:T(8,128)S(1)}) custom-call(bf16[96,1024]{1,0:T(8,128)(2,1)} %x_in.1, bf16[96,1024]{1,0:T(8,128)(2,1)} %g_in.1, bf16[352,256]{1,0:T(8,128)(2,1)} %bitcast.4, bf16[352,256]{1,0:T(8,128)(2,1)} %bitcast.5, bf16[352,256]{1,0:T(8,128)(2,1)} %wd_in.1), custom_call_target="tpu_custom_call" | custom-call | tf_op jit(solution)/shard_map/pallas_call | solution.py:542
  49.2 1.1 %shard_map.85 = (bf16[96,1024]{1,0:T(8,128)(2,1)}, f32[352,256]{1,0:T(8,128)}, f32[352,256]{1,0:T(8,128)}, f32[352,256]{1,0:T(8,128)}) custom-call(bf16[96,1024]{1,0:T(8,128)(2,1)S(1)} %get-tuple-element.12.refs_0_, f32[352,256]{1,0:T(8,128)S(1)} %get-tuple-element.13.refs_1_, f32[352,256]{1,0:T(8,128)S(1)} %get-tuple-element.14.refs_2_, ...), custom_call_target="tpu_custom_call" | custom-call | tf_op jit(solution)/shard_map/pallas_call | solution.py:574

commit v6 on v4

--- a/solution.py
+++ b/solution.py
@@ -11,7 +11,7 @@
 F32 = jnp.float32
 MESH = pl.DeviceIdType.MESH
 COPIES = 144
-SPLIT = (128, 256, 192), (128, 192, 192)
+SPLIT = (256, 128, 192), (192, 128, 192)
 
 
 def nt(left, right):
@@ -357,23 +357,39 @@
             OUTT[pl.ds(start, total.shape[0]), :] = total.astype(BF16)
 
     class Gather:
-        def __init__(self, base, count):
-            self.base, self.count = base, count // 4
+        def __init__(self, base, count, relayed):
+            self.base, self.count, self.relayed = base, count // 4, relayed
 
         def row(self, step):
             return pl.multiple_of(self.base + turn(rep, step) * self.count, 16)
 
-        def region(self, step):
-            return OUTT.at[pl.ds(self.row(step), self.count)]
+        def region(self, step, which=None):
+            rows = pl.ds(self.row(step), self.count)
+            if which is None:
+                return OUTT.at[rows]
+            return OUTT.at[rows, pl.ds(which * (shard // 2), shard // 2)]
 
         def start(self):
+            steps = (1, 3) if self.relayed else (2, 1, 3)
             self.keys = [
-                (send(self.region(0), self.region(0), at_z(step)), 4 - step) for step in (2, 1, 3)
+                (send(self.region(0), self.region(0), at_z(step)), 4 - step) for step in steps
             ]
 
+        def relay(self):
+            (right, _), (left, _) = self.keys
+            arrived(right, self.region(3))
+            first = send(self.region(3, 0), self.region(3, 0), at_z(1))
+            arrived(left, self.region(1))
+            second = send(self.region(1, 1), self.region(1, 1), at_z(3))
+            self.keys = first, second
+
         def finish(self):
-            for k, step in self.keys:
-                arrived(k, self.region(step))
+            if self.relayed:
+                for which, k in enumerate(self.keys):
+                    arrived(k, self.region(2, which))
+            else:
+                for k, step in self.keys:
+                    arrived(k, self.region(step))
 
     A, B = SPLIT
     a_at = [sum(A[:i]) for i in range(len(A))]
@@ -382,8 +398,8 @@
     zb = [Ring(z_piece(PW, r, n // 4, width // 2), bufs, at_z) for r, n, bufs in zip(b_at, B, ZB_BUFS)]
     za = [Exchange(strip(buf, n), bufs, at_z) for buf, n, bufs in zip(YA, A, ZA_BUFS)]
     yb = [Exchange(column(buf), bufs, at_y) for buf, bufs in zip(ZB, YB_BUFS)]
-    ga = [Gather(r, n) for r, n in zip(a_at, A)]
-    gb = [Gather(r, n) for r, n in zip(b_at, B)]
+    ga = [Gather(r, n, i < 2) for i, (r, n) in enumerate(zip(a_at, A))]
+    gb = [Gather(r, n, i < 2) for i, (r, n) in enumerate(zip(b_at, B))]
     xr = Ring(x_piece, XR_BUFS, at_x)
 
     def keep(buf):
@@ -429,72 +445,76 @@
     weight_rows(b_at[0], B[0])
     zb[0].start_far()
     weight_piece(1, 0, A[0])
+    zb[0].start_near()
     weight_piece(3, 0, A[0])
     ya[0].start_near()
     weight_rows(a_at[1], A[1])
-    zb[0].start_near()
     weight_rows(b_at[1], B[1])
     ya[1].start_far()
+    zb[1].start_far()
     weight_rows(a_at[2], A[2])
-    zb[1].start_far()
+    zb[1].start_near()
     weight_rows(b_at[2], B[2])
+    ya[1].start_near()
     input_piece(2)
     opp = across(OPP)
-    ya[1].start_near()
-    zb[1].start_near()
+    ya[2].start_far()
+    zb[2].start_far()
     input_piece(1)
     near = across(LEFT), across(RIGHT)
     ya[0].relay()
+    zb[0].relay()
     input_piece(0)
     mine = across(SELF)
-    zb[0].relay()
-    weight_piece(0, 0, A[0])
     across_add(opp, OPP)
     xr.start_far()
-    zb[2].start_far()
-    ya[2].start_far()
+    weight_piece(0, 0, A[0])
+    zb[2].start_near()
     across_add(near[0], LEFT)
     across_add(near[1], RIGHT)
+    zb[1].relay()
     xr.start_near()
+    ya[2].start_near()
     ya[1].relay()
-    zb[1].relay()
     across_add(mine, SELF)
-    zb[2].start_near()
+    zb[2].relay()
+    ya[2].relay()
     zb[0].finish(keep(ZB[0]))
     yb[0].start()
     ya[0].finish(keep(YA[0]))
     za[0].start()
-    ya[2].start_near()
-    zb[2].relay()
-    ya[2].relay()
     xr.relay()
     zb[1].finish(keep(ZB[1]))
     yb[1].start()
     ya[1].finish(keep(YA[1]))
     za[1].start()
+    zb[2].finish(keep(ZB[2]))
+    yb[2].start()
+    ya[2].finish(keep(YA[2]))
+    za[2].start()
     yb[0].finish(gb[0].row(0))
     gb[0].start()
     za[0].finish(ga[0].row(0))
     ga[0].start()
-    zb[2].finish(keep(ZB[2]))
-    yb[2].start()
-    ya[2].finish(keep(YA[2]))
-    za[2].start()
-    xr.finish(keep(gin_out))
     yb[1].finish(gb[1].row(0))
     gb[1].start()
+    xr.finish(keep(gin_out))
     za[1].finish(ga[1].row(0))
     ga[1].start()
-    gb[0].finish()
-    ga[0].finish()
     yb[2].finish(gb[2].row(0))
     gb[2].start()
     za[2].finish(ga[2].row(0))
     ga[2].start()
+    gb[0].relay()
+    ga[0].relay()
+    gb[1].relay()
+    ga[1].relay()
+    gb[2].finish()
+    ga[2].finish()
+    gb[0].finish()
+    ga[0].finish()
     gb[1].finish()
     ga[1].finish()
-    gb[2].finish()
-    ga[2].finish()
     og_out[...] = OUTT[pl.ds(0, hid), :].astype(F32)
     ou_out[...] = OUTT[pl.ds(hid, hid), :].astype(F32)
     od_out[...] = OUTT[pl.ds(2 * hid, hid), :].astype(F32)

time: 50.1 us -> 50.5 us (level)
  no operation moved by 1% of the time
where the time goes in v6:
time: 50.5 us; the launch traced here: 50.4 us
  Pallas kernels  49.7 us (98%)
  between operations  0.64 us (1%)
    pallas_call x1, Pallas kernels, body(): pl.pallas_call(functools.partial(kernel, factor, block, width, hid), out_...  48.6 us
    pallas_call x1, Pallas kernels, body(): pl.pallas_call(writer, out_shape=outs, in_specs=[pl.BlockSpec(memory_spac...  1.08 us

profile of v6, /device:TPU:0, one launch (start us, length us, event | category | flops | bytes accessed | tf_op | source)
XLA Modules:
  0.0 50.4 jit_solution(8476325479700573364)
XLA Ops:
  0.6 48.6 %shard_map.84 = (bf16[96,1024]{1,0:T(8,128)(2,1)S(1)}, f32[352,256]{1,0:T(8,128)S(1)}, f32[352,256]{1,0:T(8,128)S(1)}, f32[352,256]{1,0:T(8,128)S(1)}) custom-call(bf16[96,1024]{1,0:T(8,128)(2,1)} %x_in.1, bf16[96,1024]{1,0:T(8,128)(2,1)} %g_in.1, bf16[352,256]{1,0:T(8,128)(2,1)} %bitcast.4, bf16[352,256]{1,0:T(8,128)(2,1)} %bitcast.5, bf16[352,256]{1,0:T(8,128)(2,1)} %wd_in.1), custom_call_target="tpu_custom_call" | custom-call | tf_op jit(solution)/shard_map/pallas_call | solution.py:562
  49.3 1.1 %shard_map.85 = (bf16[96,1024]{1,0:T(8,128)(2,1)}, f32[352,256]{1,0:T(8,128)}, f32[352,256]{1,0:T(8,128)}, f32[352,256]{1,0:T(8,128)}) custom-call(bf16[96,1024]{1,0:T(8,128)(2,1)S(1)} %get-tuple-element.12.refs_0_, f32[352,256]{1,0:T(8,128)S(1)} %get-tuple-element.13.refs_1_, f32[352,256]{1,0:T(8,128)S(1)} %get-tuple-element.14.refs_2_, ...), custom_call_target="tpu_custom_call" | custom-call | tf_op jit(solution)/shard_map/pallas_call | solution.py:594

commit v7 on v5

--- a/solution.py
+++ b/solution.py
@@ -30,7 +30,7 @@
     factor, block, width, hid,
     x_in, g_in, wg_in, wu_in, wd_in,
     gin_out, og_out, ou_out, od_out,
-    X, G, WT, H, ACT, SLOPE, PW, DX, DS, GX, YA, ZB, OUTT, YA_BUFS, ZB_BUFS, ZA_BUFS, YB_BUFS, XR_BUFS,
+    X, G, WT, H, ACT, SLOPE, SUM, PW, DX, DS, GX, YA, ZB, OUTT, YA_BUFS, ZB_BUFS, ZA_BUFS, YB_BUFS, XR_BUFS,
     send_sems, recv_sems, local_sems,
 ):
     rep = lax.axis_index("rep")
@@ -270,6 +270,10 @@
     grad_stage(0)
     forwarded(G, g_near[1])
     grad_stage(1)
+    first = pl.ds(sum(SPLIT[0]), SPLIT[1][0])
+    early, late = pl.ds(0, 2 * 256), pl.ds(2 * 256, 256)
+    for n in range(4):
+        SUM[:, pl.ds(n * 256, 256)] = nn(H[first, early], X[early, pl.ds(n * 256, 256)])
     forwarded(G, *g_far)
     grad_stage(2)
 
@@ -406,6 +410,11 @@
                         factor * nn(H[pl.ds(lo, hi - lo), :], tokens[:, pl.ds(n * 256, 256)])
                     ).astype(BF16)
 
+    def first_rows():
+        for n in range(4):
+            lanes = pl.ds(n * 256, 256)
+            PW[first, lanes] = (factor * (SUM[:, lanes] + nn(H[first, late], X[late, lanes]))).astype(BF16)
+
     def input_piece(c):
         DX[pl.ds(c * 256, 256), :] = tn(
             H[pl.ds(0, 2 * hid), pl.ds(c * 256, 256)], WT[pl.ds(0, 2 * hid), :]
@@ -424,12 +433,12 @@
 
     blank = PW.shape[0] - 3 * hid
     PW[pl.ds(3 * hid, blank), :] = jnp.zeros((blank, width), BF16)
+    first_rows()
+    zb[0].start_far()
     weight_piece(2, 0, A[0])
     ya[0].start_far()
-    weight_rows(b_at[0], B[0])
-    zb[0].start_far()
+    zb[0].start_near()
     weight_piece(1, 0, A[0])
-    zb[0].start_near()
     weight_piece(3, 0, A[0])
     ya[0].start_near()
     weight_rows(a_at[1], A[1])
@@ -438,25 +447,25 @@
     zb[1].start_far()
     weight_rows(a_at[2], A[2])
     weight_rows(b_at[2], B[2])
-    ya[1].start_near()
     input_piece(2)
     opp = across(OPP)
-    ya[0].relay()
     zb[0].relay()
+    ya[1].start_near()
     input_piece(1)
     near = across(LEFT), across(RIGHT)
+    ya[0].relay()
     zb[1].start_near()
     input_piece(0)
     mine = across(SELF)
-    ya[2].start_far()
     weight_piece(0, 0, A[0])
     across_add(opp, OPP)
     xr.start_far()
+    ya[2].start_far()
     zb[2].start_far()
-    ya[1].relay()
-    zb[1].relay()
     across_add(near[0], LEFT)
     across_add(near[1], RIGHT)
+    zb[1].relay()
+    ya[1].relay()
     xr.start_near()
     across_add(mine, SELF)
     zb[0].finish(keep(ZB[0]))
@@ -465,8 +474,8 @@
     ya[2].start_near()
     ya[0].finish(keep(YA[0]))
     za[0].start()
+    zb[2].relay()
     ya[2].relay()
-    zb[2].relay()
     xr.relay()
     ya[1].finish(keep(YA[1]))
     za[1].start()
@@ -476,15 +485,15 @@
     gb[0].start()
     za[0].finish(ga[0].row(0))
     ga[0].start()
+    zb[2].finish(keep(ZB[2]))
+    yb[2].start()
     ya[2].finish(keep(YA[2]))
     za[2].start()
-    zb[2].finish(keep(ZB[2]))
-    yb[2].start()
     za[1].finish(ga[1].row(0))
     ga[1].start()
+    xr.finish(keep(gin_out))
     yb[1].finish(gb[1].row(0))
     gb[1].start()
-    xr.finish(keep(gin_out))
     gb[0].finish()
     ga[0].finish()
     yb[2].finish(gb[2].row(0))
@@ -551,6 +560,7 @@
             pltpu.VMEM((3 * hid, tokens), BF16),
             pltpu.VMEM((hid, tokens), F32),
             pltpu.VMEM((hid, tokens), F32),
+            pltpu.VMEM((B[0], width), F32),
             pltpu.VMEM((total_rows, width), BF16),
             pltpu.VMEM((tokens, width), BF16),
             pltpu.VMEM((tokens // 2, width), BF16),

time: 50.4 us -> 50.4 us (level)
  no operation moved by 1% of the time
where the time goes in v7:
time: 50.4 us; the launch traced here: 50.2 us
  Pallas kernels  49.6 us (98%)
  between operations  0.64 us (1%)
    pallas_call x1, Pallas kernels, body(): pl.pallas_call(functools.partial(kernel, factor, block, width, hid), out_...  48.5 us
    pallas_call x1, Pallas kernels, body(): pl.pallas_call(writer, out_shape=outs, in_specs=[pl.BlockSpec(memory_spac...  1.08 us

profile of v7, /device:TPU:0, one launch (start us, length us, event | category | flops | bytes accessed | tf_op | source)
XLA Modules:
  0.0 50.2 jit_solution(12771935377359670389)
XLA Ops:
  0.6 48.5 %shard_map.84 = (bf16[96,1024]{1,0:T(8,128)(2,1)S(1)}, f32[352,256]{1,0:T(8,128)S(1)}, f32[352,256]{1,0:T(8,128)S(1)}, f32[352,256]{1,0:T(8,128)S(1)}) custom-call(bf16[96,1024]{1,0:T(8,128)(2,1)} %x_in.1, bf16[96,1024]{1,0:T(8,128)(2,1)} %g_in.1, bf16[352,256]{1,0:T(8,128)(2,1)} %bitcast.4, bf16[352,256]{1,0:T(8,128)(2,1)} %bitcast.5, bf16[352,256]{1,0:T(8,128)(2,1)} %wd_in.1), custom_call_target="tpu_custom_call" | custom-call | tf_op jit(solution)/shard_map/pallas_call | solution.py:551
  49.2 1.1 %shard_map.85 = (bf16[96,1024]{1,0:T(8,128)(2,1)}, f32[352,256]{1,0:T(8,128)}, f32[352,256]{1,0:T(8,128)}, f32[352,256]{1,0:T(8,128)}) custom-call(bf16[96,1024]{1,0:T(8,128)(2,1)S(1)} %get-tuple-element.12.refs_0_, f32[352,256]{1,0:T(8,128)S(1)} %get-tuple-element.13.refs_1_, f32[352,256]{1,0:T(8,128)S(1)} %get-tuple-element.14.refs_2_, ...), custom_call_target="tpu_custom_call" | custom-call | tf_op jit(solution)/shard_map/pallas_call | solution.py:584

commit v8 on v7

--- a/solution.py
+++ b/solution.py
@@ -435,71 +435,71 @@
     PW[pl.ds(3 * hid, blank), :] = jnp.zeros((blank, width), BF16)
     first_rows()
     zb[0].start_far()
+    zb[0].start_near()
     weight_piece(2, 0, A[0])
     ya[0].start_far()
-    zb[0].start_near()
+    weight_rows(b_at[1], B[1])
+    zb[1].start_far()
     weight_piece(1, 0, A[0])
     weight_piece(3, 0, A[0])
     ya[0].start_near()
     weight_rows(a_at[1], A[1])
-    weight_rows(b_at[1], B[1])
     ya[1].start_far()
-    zb[1].start_far()
+    zb[1].start_near()
+    weight_rows(b_at[2], B[2])
+    zb[2].start_far()
     weight_rows(a_at[2], A[2])
-    weight_rows(b_at[2], B[2])
+    ya[1].start_near()
+    ya[2].start_far()
     input_piece(2)
     opp = across(OPP)
     zb[0].relay()
-    ya[1].start_near()
     input_piece(1)
     near = across(LEFT), across(RIGHT)
     ya[0].relay()
-    zb[1].start_near()
     input_piece(0)
     mine = across(SELF)
     weight_piece(0, 0, A[0])
     across_add(opp, OPP)
     xr.start_far()
-    ya[2].start_far()
-    zb[2].start_far()
+    zb[1].relay()
+    zb[2].start_near()
     across_add(near[0], LEFT)
     across_add(near[1], RIGHT)
-    zb[1].relay()
+    xr.start_near()
     ya[1].relay()
-    xr.start_near()
+    ya[2].start_near()
     across_add(mine, SELF)
+    zb[2].relay()
     zb[0].finish(keep(ZB[0]))
     yb[0].start()
-    zb[2].start_near()
-    ya[2].start_near()
+    ya[2].relay()
     ya[0].finish(keep(YA[0]))
     za[0].start()
-    zb[2].relay()
-    ya[2].relay()
-    xr.relay()
+    zb[1].finish(keep(ZB[1]))
+    yb[1].start()
     ya[1].finish(keep(YA[1]))
     za[1].start()
-    zb[1].finish(keep(ZB[1]))
-    yb[1].start()
+    zb[2].finish(keep(ZB[2]))
+    yb[2].start()
+    xr.relay()
     yb[0].finish(gb[0].row(0))
     gb[0].start()
+    ya[2].finish(keep(YA[2]))
+    za[2].start()
     za[0].finish(ga[0].row(0))
     ga[0].start()
-    zb[2].finish(keep(ZB[2]))
-    yb[2].start()
-    ya[2].finish(keep(YA[2]))
-    za[2].start()
     za[1].finish(ga[1].row(0))
     ga[1].start()
-    xr.finish(keep(gin_out))
     yb[1].finish(gb[1].row(0))
     gb[1].start()
-    gb[0].finish()
-    ga[0].finish()
     yb[2].finish(gb[2].row(0))
     gb[2].start()
     za[2].finish(ga[2].row(0))
     ga[2].start()
+    xr.finish(keep(gin_out))
+    gb[0].finish()
+    ga[0].finish()
     ga[1].finish()
     gb[1].finish()
     gb[2].finish()

time: 50.4 us -> 50.9 us (level)
  Pallas kernels: 49.6 us -> 50.2 us
    pallas_call x1, Pallas kernels: 48.5 us -> 49.1 us  [body(): pl.pallas_call(functools.partial(kernel, factor, block, width, hid), out_...]
where the time goes in v8:
time: 50.9 us; the launch traced here: 50.8 us
  Pallas kernels  50.2 us (99%)
  between operations  0.64 us (1%)
    pallas_call x1, Pallas kernels, body(): pl.pallas_call(functools.partial(kernel, factor, block, width, hid), out_...  49.1 us
    pallas_call x1, Pallas kernels, body(): pl.pallas_call(writer, out_shape=outs, in_specs=[pl.BlockSpec(memory_spac...  1.08 us

profile of v8, /device:TPU:0, one launch (start us, length us, event | category | flops | bytes accessed | tf_op | source)
XLA Modules:
  0.0 50.8 jit_solution(14752763584975346770)
XLA Ops:
  0.6 49.1 %shard_map.84 = (bf16[96,1024]{1,0:T(8,128)(2,1)S(1)}, f32[352,256]{1,0:T(8,128)S(1)}, f32[352,256]{1,0:T(8,128)S(1)}, f32[352,256]{1,0:T(8,128)S(1)}) custom-call(bf16[96,1024]{1,0:T(8,128)(2,1)} %x_in.1, bf16[96,1024]{1,0:T(8,128)(2,1)} %g_in.1, bf16[352,256]{1,0:T(8,128)(2,1)} %bitcast.4, bf16[352,256]{1,0:T(8,128)(2,1)} %bitcast.5, bf16[352,256]{1,0:T(8,128)(2,1)} %wd_in.1), custom_call_target="tpu_custom_call" | custom-call | tf_op jit(solution)/shard_map/pallas_call | solution.py:551
  49.8 1.1 %shard_map.85 = (bf16[96,1024]{1,0:T(8,128)(2,1)}, f32[352,256]{1,0:T(8,128)}, f32[352,256]{1,0:T(8,128)}, f32[352,256]{1,0:T(8,128)}) custom-call(bf16[96,1024]{1,0:T(8,128)(2,1)S(1)} %get-tuple-element.12.refs_0_, f32[352,256]{1,0:T(8,128)S(1)} %get-tuple-element.13.refs_1_, f32[352,256]{1,0:T(8,128)S(1)} %get-tuple-element.14.refs_2_, ...), custom_call_target="tpu_custom_call" | custom-call | tf_op jit(solution)/shard_map/pallas_call | solution.py:584

commit v9 on v4

--- a/solution.py
+++ b/solution.py
@@ -442,12 +442,12 @@
     opp = across(OPP)
     ya[1].start_near()
     zb[1].start_near()
+    ya[0].relay()
+    zb[0].relay()
     input_piece(1)
     near = across(LEFT), across(RIGHT)
-    ya[0].relay()
     input_piece(0)
     mine = across(SELF)
-    zb[0].relay()
     weight_piece(0, 0, A[0])
     across_add(opp, OPP)
     xr.start_far()

time: 50.1 us -> 50.5 us (level)
  no operation moved by 1% of the time
where the time goes in v9:
time: 50.5 us; the launch traced here: 50.4 us
  Pallas kernels  49.7 us (98%)
  between operations  0.64 us (1%)
    pallas_call x1, Pallas kernels, body(): pl.pallas_call(functools.partial(kernel, factor, block, width, hid), out_...  48.7 us
    pallas_call x1, Pallas kernels, body(): pl.pallas_call(writer, out_shape=outs, in_specs=[pl.BlockSpec(memory_spac...  1.08 us

profile of v9, /device:TPU:0, one launch (start us, length us, event | category | flops | bytes accessed | tf_op | source)
XLA Modules:
  0.0 50.4 jit_solution(16053597263618187220)
XLA Ops:
  0.6 48.7 %shard_map.84 = (bf16[96,1024]{1,0:T(8,128)(2,1)S(1)}, f32[352,256]{1,0:T(8,128)S(1)}, f32[352,256]{1,0:T(8,128)S(1)}, f32[352,256]{1,0:T(8,128)S(1)}) custom-call(bf16[96,1024]{1,0:T(8,128)(2,1)} %x_in.1, bf16[96,1024]{1,0:T(8,128)(2,1)} %g_in.1, bf16[352,256]{1,0:T(8,128)(2,1)} %bitcast.4, bf16[352,256]{1,0:T(8,128)(2,1)} %bitcast.5, bf16[352,256]{1,0:T(8,128)(2,1)} %wd_in.1), custom_call_target="tpu_custom_call" | custom-call | tf_op jit(solution)/shard_map/pallas_call | solution.py:542
  49.3 1.1 %shard_map.85 = (bf16[96,1024]{1,0:T(8,128)(2,1)}, f32[352,256]{1,0:T(8,128)}, f32[352,256]{1,0:T(8,128)}, f32[352,256]{1,0:T(8,128)}) custom-call(bf16[96,1024]{1,0:T(8,128)(2,1)S(1)} %get-tuple-element.12.refs_0_, f32[352,256]{1,0:T(8,128)S(1)} %get-tuple-element.13.refs_1_, f32[352,256]{1,0:T(8,128)S(1)} %get-tuple-element.14.refs_2_, ...), custom_call_target="tpu_custom_call" | custom-call | tf_op jit(solution)/shard_map/pallas_call | solution.py:574

commit v10 on v4

--- a/solution.py
+++ b/solution.py
@@ -494,12 +494,13 @@
     gb[1].finish()
     ga[1].finish()
     gb[2].finish()
+    og_out[...] = OUTT[pl.ds(0, hid), :].astype(F32)
+    od_out[...] = OUTT[pl.ds(2 * hid, hid), :].astype(F32)
+    for copy in pending[:-3]:
+        copy.wait_send()
     ga[2].finish()
-    og_out[...] = OUTT[pl.ds(0, hid), :].astype(F32)
     ou_out[...] = OUTT[pl.ds(hid, hid), :].astype(F32)
-    od_out[...] = OUTT[pl.ds(2 * hid, hid), :].astype(F32)
-
-    for copy in pending:
+    for copy in pending[-3:]:
         copy.wait_send()
 
 

time: 50.1 us -> 49.8 us (level)
  no operation moved by 1% of the time
where the time goes in v10:
time: 49.8 us; the launch traced here: 49.7 us
  Pallas kernels  49.1 us (99%)
  between operations  0.64 us (1%)
    pallas_call x1, Pallas kernels, body(): pl.pallas_call(functools.partial(kernel, factor, block, width, hid), out_...  48 us
    pallas_call x1, Pallas kernels, body(): pl.pallas_call(writer, out_shape=outs, in_specs=[pl.BlockSpec(memory_spac...  1.08 us

profile of v10, /device:TPU:0, one launch (start us, length us, event | category | flops | bytes accessed | tf_op | source)
XLA Modules:
  0.0 49.7 jit_solution(3133291345636895193)
XLA Ops:
  0.6 48.0 %shard_map.84 = (bf16[96,1024]{1,0:T(8,128)(2,1)S(1)}, f32[352,256]{1,0:T(8,128)S(1)}, f32[352,256]{1,0:T(8,128)S(1)}, f32[352,256]{1,0:T(8,128)S(1)}) custom-call(bf16[96,1024]{1,0:T(8,128)(2,1)} %x_in.1, bf16[96,1024]{1,0:T(8,128)(2,1)} %g_in.1, bf16[352,256]{1,0:T(8,128)(2,1)} %bitcast.4, bf16[352,256]{1,0:T(8,128)(2,1)} %bitcast.5, bf16[352,256]{1,0:T(8,128)(2,1)} %wd_in.1), custom_call_target="tpu_custom_call" | custom-call | tf_op jit(solution)/shard_map/pallas_call | solution.py:543
  48.6 1.1 %shard_map.85 = (bf16[96,1024]{1,0:T(8,128)(2,1)}, f32[352,256]{1,0:T(8,128)}, f32[352,256]{1,0:T(8,128)}, f32[352,256]{1,0:T(8,128)}) custom-call(bf16[96,1024]{1,0:T(8,128)(2,1)S(1)} %get-tuple-element.12.refs_0_, f32[352,256]{1,0:T(8,128)S(1)} %get-tuple-element.13.refs_1_, f32[352,256]{1,0:T(8,128)S(1)} %get-tuple-element.14.refs_2_, ...), custom_call_target="tpu_custom_call" | custom-call | tf_op jit(solution)/shard_map/pallas_call | solution.py:575

commit v11 on v10

--- a/solution.py
+++ b/solution.py
@@ -258,8 +258,8 @@
         H[pl.ds(hid, hid), cols] = (grad * ACT[:, cols]).astype(BF16)
 
     gate_stage(0)
+    g_near = gt.near()
     gate_stage(1)
-    g_near = gt.near()
     forwarded(X, *x_far)
     gate_stage(2)
     q2.finish()

time: 49.8 us -> 50.4 us (1.012)
    pallas_call x1, Pallas kernels: 48 us -> 48.5 us  [body(): pl.pallas_call(functools.partial(kernel, factor, block, width, hid), out_...]
where the time goes in v11:
time: 50.4 us; the launch traced here: 50.3 us
  Pallas kernels  49.6 us (98%)
  between operations  0.64 us (1%)
    pallas_call x1, Pallas kernels, body(): pl.pallas_call(functools.partial(kernel, factor, block, width, hid), out_...  48.5 us
    pallas_call x1, Pallas kernels, body(): pl.pallas_call(writer, out_shape=outs, in_specs=[pl.BlockSpec(memory_spac...  1.08 us

profile of v11, /device:TPU:0, one launch (start us, length us, event | category | flops | bytes accessed | tf_op | source)
XLA Modules:
  0.0 50.3 jit_solution(236420139080595583)
XLA Ops:
  0.6 48.5 %shard_map.84 = (bf16[96,1024]{1,0:T(8,128)(2,1)S(1)}, f32[352,256]{1,0:T(8,128)S(1)}, f32[352,256]{1,0:T(8,128)S(1)}, f32[352,256]{1,0:T(8,128)S(1)}) custom-call(bf16[96,1024]{1,0:T(8,128)(2,1)} %x_in.1, bf16[96,1024]{1,0:T(8,128)(2,1)} %g_in.1, bf16[352,256]{1,0:T(8,128)(2,1)} %bitcast.4, bf16[352,256]{1,0:T(8,128)(2,1)} %bitcast.5, bf16[352,256]{1,0:T(8,128)(2,1)} %wd_in.1), custom_call_target="tpu_custom_call" | custom-call | tf_op jit(solution)/shard_map/pallas_call | solution.py:543
  49.2 1.1 %shard_map.85 = (bf16[96,1024]{1,0:T(8,128)(2,1)}, f32[352,256]{1,0:T(8,128)}, f32[352,256]{1,0:T(8,128)}, f32[352,256]{1,0:T(8,128)}) custom-call(bf16[96,1024]{1,0:T(8,128)(2,1)S(1)} %get-tuple-element.12.refs_0_, f32[352,256]{1,0:T(8,128)S(1)} %get-tuple-element.13.refs_1_, f32[352,256]{1,0:T(8,128)S(1)} %get-tuple-element.14.refs_2_, ...), custom_call_target="tpu_custom_call" | custom-call | tf_op jit(solution)/shard_map/pallas_call | solution.py:575

commit v12 on v10

--- a/solution.py
+++ b/solution.py
@@ -266,8 +266,8 @@
     for k, step in d2:
         arrived(k, w(D2, step))
     forwarded(G, g_own, g_near[0])
+    grad_stage(0)
     g_far = gt.far()
-    grad_stage(0)
     forwarded(G, g_near[1])
     grad_stage(1)
     forwarded(G, *g_far)

time: 49.8 us -> 50.6 us (1.016)
  Pallas kernels: 49.1 us -> 49.8 us
    pallas_call x1, Pallas kernels: 48 us -> 48.8 us  [body(): pl.pallas_call(functools.partial(kernel, factor, block, width, hid), out_...]
where the time goes in v12:
time: 50.6 us; the launch traced here: 50.5 us
  Pallas kernels  49.8 us (98%)
  between operations  0.64 us (1%)
    pallas_call x1, Pallas kernels, body(): pl.pallas_call(functools.partial(kernel, factor, block, width, hid), out_...  48.8 us
    pallas_call x1, Pallas kernels, body(): pl.pallas_call(writer, out_shape=outs, in_specs=[pl.BlockSpec(memory_spac...  1.08 us

profile of v12, /device:TPU:0, one launch (start us, length us, event | category | flops | bytes accessed | tf_op | source)
XLA Modules:
  0.0 50.5 jit_solution(9080958445455139734)
XLA Ops:
  0.6 48.8 %shard_map.84 = (bf16[96,1024]{1,0:T(8,128)(2,1)S(1)}, f32[352,256]{1,0:T(8,128)S(1)}, f32[352,256]{1,0:T(8,128)S(1)}, f32[352,256]{1,0:T(8,128)S(1)}) custom-call(bf16[96,1024]{1,0:T(8,128)(2,1)} %x_in.1, bf16[96,1024]{1,0:T(8,128)(2,1)} %g_in.1, bf16[352,256]{1,0:T(8,128)(2,1)} %bitcast.4, bf16[352,256]{1,0:T(8,128)(2,1)} %bitcast.5, bf16[352,256]{1,0:T(8,128)(2,1)} %wd_in.1), custom_call_target="tpu_custom_call" | custom-call | tf_op jit(solution)/shard_map/pallas_call | solution.py:543
  49.4 1.1 %shard_map.85 = (bf16[96,1024]{1,0:T(8,128)(2,1)}, f32[352,256]{1,0:T(8,128)}, f32[352,256]{1,0:T(8,128)}, f32[352,256]{1,0:T(8,128)}) custom-call(bf16[96,1024]{1,0:T(8,128)(2,1)S(1)} %get-tuple-element.12.refs_0_, f32[352,256]{1,0:T(8,128)S(1)} %get-tuple-element.13.refs_1_, f32[352,256]{1,0:T(8,128)S(1)} %get-tuple-element.14.refs_2_, ...), custom_call_target="tpu_custom_call" | custom-call | tf_op jit(solution)/shard_map/pallas_call | solution.py:575
